TPU v7x, 32 devices: a whole 2x2x4 slice. The times are simulated.
32 devices in a mesh: grp: 2 (over y), ep: 4 (over z), tp: 4 (over x, core).
Axes of the slice: x: 2, y: 2, z: 4, core: 2. Of those that a mesh axis runs over, the one named last changes fastest.
Arguments:
- mix_input: bfloat16 [2048, 2048], P(('grp', 'ep'), 'tp'), parts along dimension 0, may hold values from -6 to 6
- group_weight: bfloat16 [16, 128, 128], replicated, may hold values from -0.5 to 0.5
- pool_gain: float32 [2048], replicated, may hold values from 0.1 to 1.9
- branch_weight: bfloat16 [2048, 2048], P('tp'), may hold values from -0.125 to 0.125
- exp_input: bfloat16 [1024, 2048], P(('grp', 'ep')), parts along dimension 0, may hold values from -6 to 6
- norm_gain: float32 [2048], replicated, may hold values from 0.1 to 1.9
- routes: int32 [1024, 2], P(('grp', 'ep')), parts along dimension 0, may hold values from 0 to 3, all different within a row; in each aligned block of 128 rows (0 to 127, 128 to 255, ...) at most 96 rows name the same one
- route_weights: float32 [1024, 2], P(('grp', 'ep')), parts along dimension 0, may hold values from 0.25 to 1
- gate_weight: bfloat16 [4, 2048, 3584], P('ep', None, 'tp'), may hold values from -0.125 to 0.125
- up_weight: bfloat16 [4, 2048, 3584], P('ep', None, 'tp'), may hold values from -0.125 to 0.125
- down_weight: bfloat16 [4, 3584, 2048], P('ep', 'tp'), may hold values from -0.09375 to 0.09375
Outputs:
- mix_out: bfloat16 [2048, 2048], P(('grp', 'ep'), 'tp'), parts along dimension 0
- exp_out: bfloat16 [1024, 2048], P(('grp', 'ep'), 'tp'), parts along dimension 0
There are 2 independent parts, one for each index of `grp`. A program takes and returns all parts, laid end to end along the dimension named above; an argument that names none is the same for every part. Nothing has to cross between parts.
Inputs may be any that keep to these rules, and one draw needn't show every extreme that they name: `routes`: the 2 experts of a token differ. Among the 128 tokens of one index of ep no expert is named by more than 96 of them, a bound that some block reaches.
All inputs are finite; a program needn't handle non-finite values.
Results may differ from a plain program's by a relative error of at most 0.018.
Values may be sent and summed in bfloat16 or wider, within the bound.
A program may use at most 64 MiB of HBM per device.

v0:
```python
import functools

import jax
import jax.numpy as jnp
from jax import lax
from jax.experimental import pallas as pl
from jax.experimental.pallas import tpu as pltpu
from jax.sharding import PartitionSpec as P

windows = (2, 4, 8, 16)
epsilon = 1e-06


def shifted(block, axis, distance):
    devices = range(lax.axis_size(axis))
    route = [(i - distance, i) for i in devices if i - distance in devices]
    return lax.ppermute(block, axis, route)


def trailing_sums(extended, rows):
    span_two = extended[1:] + extended[:-1]
    span_four = span_two[2:] + span_two[:-2]
    span_eight = span_four[4:] + span_four[:-4]
    span_sixteen = span_eight[8:] + span_eight[:-8]
    return [span_two[-rows:], span_four[-rows:], span_eight[-rows:], span_sixteen]


def pooled_deviation(extended, positions, group_ids, group_width, rows):
    sums = trailing_sums(extended, rows)
    current = extended[-rows:]
    window_id = jnp.repeat(group_ids % 4, group_width)
    result = jnp.zeros_like(current)
    for window_level, window_len in enumerate(windows):
        counted = jnp.minimum(positions + 1, window_len).astype(jnp.float32)[:, None]
        result = jnp.where(
            window_id[None, :] == window_level, sums[window_level] / counted - current, result
        )
    return result


def on_device(
    mix_input,
    group_weight,
    pool_gain,
    branch_weight,
    exp_input,
    norm_gain,
    routes,
    route_weights,
    gate_weight,
    up_weight,
    down_weight,
):
    tp_rank = lax.axis_index("tp")
    ep_rank = lax.axis_index("ep")
    rows_mix, channels = mix_input.shape
    group_width = group_weight.shape[1]
    group_count = channels // group_width
    first_group = tp_rank * group_count
    last_rows = mix_input[rows_mix - 15 :]
    before = shifted(last_rows, "ep", 1)
    extended = jnp.concatenate([before, mix_input], axis=0).astype(jnp.float32)
    positions = ep_rank * rows_mix + jnp.arange(rows_mix, dtype=jnp.int32)
    group_ids = first_group + jnp.arange(group_count, dtype=jnp.int32)
    deviation = pooled_deviation(extended, positions, group_ids, group_width, rows_mix).astype(
        jnp.bfloat16
    )
    own_groups = lax.dynamic_slice_in_dim(group_weight, first_group, group_count, 0)
    grouped = jnp.einsum(
        "rgc,gcd->rgd",
        deviation.reshape(rows_mix, group_count, group_width),
        own_groups,
        preferred_element_type=jnp.float32,
    ).reshape(rows_mix, channels)
    own_gain = lax.dynamic_slice_in_dim(pool_gain, first_group * group_width, channels, 0)
    pooled = (grouped * own_gain).astype(jnp.bfloat16)
    tok_rows, width = exp_input.shape
    columns = width // lax.axis_size("tp")
    experts_all = lax.axis_size("ep")
    capacity = 3 * tok_rows // experts_all
    floated = exp_input.astype(jnp.float32)
    normed = (
        floated
        * lax.rsqrt(jnp.mean(floated * floated, axis=1, keepdims=True) + epsilon)
        * norm_gain
    ).astype(jnp.bfloat16)
    flat_expert = routes.reshape(-1)
    assignments = flat_expert.shape[0]
    onehot = (flat_expert[:, None] == jnp.arange(experts_all, dtype=jnp.int32)[None, :]).astype(
        jnp.int32
    )
    slot_rank = jnp.sum((jnp.cumsum(onehot, axis=0) - onehot) * onehot, axis=1)
    slot_index = flat_expert * capacity + slot_rank
    token_of = jnp.arange(assignments, dtype=jnp.int32) // routes.shape[1]
    slot_token = (
        jnp.full((experts_all * capacity,), tok_rows, jnp.int32).at[slot_index].set(token_of)
    )
    padded = jnp.concatenate([normed, jnp.zeros((1, width), jnp.bfloat16)], axis=0)
    w_gate = gate_weight[0]
    w_up = up_weight[0]
    w_down = down_weight[0]
    arrived_rows = experts_all * capacity
    own_columns = lax.dynamic_slice_in_dim(padded, tp_rank * columns, columns, 1)
    outgoing = own_columns[slot_token].reshape(experts_all, capacity, columns)
    arrived = lax.all_to_all(outgoing, "ep", split_axis=0, concat_axis=0, tiled=True).reshape(
        arrived_rows, columns
    )
    section = lax.all_gather(arrived, "tp", axis=1, tiled=True)
    gate_pre = jnp.dot(section, w_gate, preferred_element_type=jnp.float32)
    up_pre = jnp.dot(section, w_up, preferred_element_type=jnp.float32)
    hidden = (jax.nn.silu(gate_pre) * up_pre).astype(jnp.bfloat16)
    weight_cols = branch_weight
    mix_sum = lax.psum_scatter(
        lax.dot_general(
            weight_cols, pooled, (((0,), (1,)), ((), ())), preferred_element_type=jnp.float32
        ).astype(jnp.bfloat16),
        "tp",
        scatter_dimension=0,
        tiled=True,
    )
    weight_cols = w_down
    exp_sum = lax.psum_scatter(
        lax.dot_general(
            weight_cols, hidden, (((0,), (1,)), ((), ())), preferred_element_type=jnp.float32
        ).astype(jnp.bfloat16),
        "tp",
        scatter_dimension=0,
        tiled=True,
    )
    mix_out = mix_sum.T
    results = exp_sum.reshape(columns, experts_all, capacity)
    returned = lax.all_to_all(results, "ep", split_axis=1, concat_axis=1, tiled=True).reshape(
        columns, experts_all * capacity
    )
    picked = returned[:, slot_index].astype(jnp.float32)
    weighted = picked * route_weights.reshape(-1)[None, :]
    combined = jnp.sum(weighted.reshape(columns, tok_rows, routes.shape[1]), axis=2)
    exp_out = combined.T.astype(jnp.bfloat16)
    return (mix_out, exp_out)


lanes = 128
MESH = pl.DeviceIdType.MESH
f32 = jnp.float32
bf16 = jnp.bfloat16


def fused_kernel(
    x_ref,
    norm_ref,
    routes_ref,
    weights_ref,
    mix_ref,
    gain_ref,
    groups_hbm,
    branch_hbm,
    gate_hbm,
    up_hbm,
    down_hbm,
    mix_out,
    exp_out,
    wgu,
    wd,
    wb,
    gw,
    xn,
    sb,
    xg,
    gu,
    hid,
    halo,
    pooled,
    keep_m,
    ps_m,
    pr_m,
    xs_m,
    xr_m,
    keep,
    ps,
    pr,
    xs,
    xr,
    zs,
    zr,
    w_sem,
    d_send,
    d_recv,
    r_send,
    r_recv,
    z_send,
    z_recv,
    m_send,
    m_recv,
    h_sem,
):
    z = lax.axis_index("ep")
    t = lax.axis_index("tp")
    near = t + 1 - 2 * (t % 2)
    across = (t + 2) % 4
    diagonal = (near + 2) % 4
    peers = [z, z + 1 - 2 * (z % 2), 3 - z, (z + 2) % 4]
    tokens, width = x_ref.shape
    quarter = width // 4
    cap = xg.shape[2]
    hid_tiles = gate_hbm.shape[2] // lanes
    rows_mix, channels = mix_ref.shape
    group_count = channels // lanes

    loads = []
    for i in range(2 * hid_tiles):
        src = gate_hbm if i < hid_tiles else up_hbm
        at = (i % hid_tiles) * lanes
        loads.append(
            pltpu.make_async_copy(
                src.at[0, :, pl.ds(at, lanes)],
                wgu.at[i // 2, :, pl.ds((i % 2) * lanes, lanes)],
                w_sem.at[i],
            )
        )
    n0 = 2 * hid_tiles
    load_b = [
        pltpu.make_async_copy(branch_hbm.at[:, pl.ds(k * quarter, quarter)], wb.at[k], w_sem.at[n0 + k])
        for k in range(4)
    ]
    load_d = [
        pltpu.make_async_copy(down_hbm.at[0, :, pl.ds(k * quarter, quarter)], wd.at[k], w_sem.at[n0 + 4 + k])
        for k in range(4)
    ]
    load_g = pltpu.make_async_copy(groups_hbm.at[pl.ds(t * group_count, group_count)], gw, w_sem.at[n0 + 8])
    load_g.start()
    for c in load_b + loads + load_d:
        c.start()

    barrier = pltpu.get_barrier_semaphore()
    for k in (1, 2, 3):
        pl.semaphore_signal(barrier, inc=1, device_id={"ep": peers[k]}, device_id_type=MESH)
    for k in (near, across):
        pl.semaphore_signal(barrier, inc=1, device_id={"tp": k}, device_id_type=MESH)

    def remote(src, dst, send, recv, who):
        return pltpu.make_async_remote_copy(
            src_ref=src, dst_ref=dst, send_sem=send, recv_sem=recv, device_id=who, device_id_type=MESH
        )

    floated = x_ref[...].astype(f32)
    scale = lax.rsqrt(jnp.mean(floated * floated, axis=1, keepdims=True) + epsilon)
    xn_val = (floated * scale * norm_ref[...]).astype(bf16)
    for k in range(4):
        xn[k] = xn_val[:, k * quarter : (k + 1) * quarter]
    lane = lax.broadcasted_iota(jnp.int32, (tokens, lanes), 1)
    square = (tokens, tokens)
    diagonal_mask = lax.broadcasted_iota(jnp.int32, square, 0) == lax.broadcasted_iota(jnp.int32, square, 1)

    def column(row):
        spread = jnp.broadcast_to(row, square)
        return jnp.sum(jnp.where(diagonal_mask, spread, jnp.zeros_like(spread)), axis=1, keepdims=True)

    r0 = column(routes_ref[0:1, :].astype(f32)).astype(jnp.int32)
    r1 = column(routes_ref[1:2, :].astype(f32)).astype(jnp.int32)
    w0 = column(weights_ref[0:1, :])
    w1 = column(weights_ref[1:2, :])
    member = ((r0 == lane) | (r1 == lane)).astype(f32)
    above = (
        lax.broadcasted_iota(jnp.int32, (tokens, tokens), 0)
        > lax.broadcasted_iota(jnp.int32, (tokens, tokens), 1)
    ).astype(f32)
    rank = jnp.dot(above.astype(bf16), member.astype(bf16), preferred_element_type=f32)
    slot_lane = lax.broadcasted_iota(jnp.int32, (tokens, cap), 1)
    places = []
    shares = []
    for k in range(4):
        own = jnp.sum(jnp.where(lane == peers[k], rank, 0.0), axis=1, keepdims=True).astype(jnp.int32)
        named = (r0 == peers[k]) | (r1 == peers[k])
        slot = jnp.where(named, own, cap)
        places.append((slot_lane == slot).astype(f32).astype(bf16))
        shares.append(
            jnp.where(r0 == peers[k], w0, 0.0)
            + jnp.where(r1 == peers[k], w1, 0.0)
        )

    def gathered(k, block):
        return lax.dot_general(
            places[k], block, (((0,), (0,)), ((), ())), preferred_element_type=f32
        ).astype(bf16)

    own_cols = xn[t]
    for k in (1, 2, 3):
        sb[k] = gathered(k, own_cols)
    pl.semaphore_wait(barrier, 5)
    halo_copy = remote(
        mix_ref.at[pl.ds(rows_mix - 16, 16), :], halo, h_sem.at[0], h_sem.at[1], {"ep": (z + 1) % 4}
    )

    @pl.when(z < 3)
    def _():
        halo_copy.start()

    d_z = []
    for k in (1, 2, 3):
        c = remote(sb.at[k], xg.at[t, k], d_send.at[k - 1, 0], d_recv.at[k - 1, 0], {"ep": peers[k]})
        c.start()
        d_z.append(c)
    for q in range(4):
        xg[q, 0] = gathered(0, xn[q])

    @pl.when(z == 0)
    def _():
        halo[...] = jnp.zeros_like(halo)

    @pl.when(z > 0)
    def _():
        halo_copy.wait_recv()

    load_g.wait()
    position = z * rows_mix + lax.broadcasted_iota(jnp.int32, (rows_mix, lanes), 0)
    for g in range(group_count):
        cols = slice(g * lanes, (g + 1) * lanes)
        current = mix_ref[:, cols].astype(f32)
        total = jnp.concatenate([halo[:, cols].astype(f32), current], axis=0)
        level = g % 4
        for step in range(level + 1):
            total = total + pltpu.roll(total, 1 << step, 0)
        counted = jnp.minimum(position + 1, windows[level]).astype(f32)
        deviation = (total[16:] / counted - current).astype(bf16)
        grouped = jnp.dot(deviation, gw[g], preferred_element_type=f32)
        gain = gain_ref[:, pl.ds(pl.multiple_of(t * channels + g * lanes, lanes), lanes)]
        pooled[:, cols] = (grouped * gain).astype(bf16)
    for c in load_b:
        c.wait()

    m_p = []
    for i, q in enumerate((diagonal, near)):
        ps_m[i] = jnp.dot(pooled[...], wb[q], preferred_element_type=f32).astype(bf16)
        c = remote(ps_m.at[i], pr_m.at[i], m_send.at[i], m_recv.at[i], {"tp": near})
        c.start()
        m_p.append(c)
    for i, q in enumerate((across, t)):
        keep_m[i] = jnp.dot(pooled[...], wb[q], preferred_element_type=f32)

    d_x = [
        remote(xg.at[t, k], xg.at[t, k], d_send.at[k - 1, 1], d_recv.at[k - 1, 1], {"tp": across})
        for k in (1, 2, 3)
    ]
    d_p = [
        remote(xg.at[t, k], xg.at[t, k], d_send.at[k - 1, 2], d_recv.at[k - 1, 2], {"tp": near})
        for k in (1, 2, 3)
    ]
    d_q = [
        remote(xg.at[across, k], xg.at[across, k], d_send.at[k - 1, 3], d_recv.at[k - 1, 3], {"tp": near})
        for k in (1, 2, 3)
    ]

    def from_z(k):
        d_z[k - 1].wait_recv()
        d_x[k - 1].start()
        d_p[k - 1].start()

    def from_x(k):
        d_x[k - 1].wait_recv()
        d_q[k - 1].start()

    def from_near(k):
        d_p[k - 1].wait_recv()
        d_q[k - 1].wait_recv()

    def expand(k, first, last):
        def tile(n, carry):
            total = None
            for q in range(4):
                part = jnp.dot(
                    xg[q, k], wgu[n, q * quarter : (q + 1) * quarter, :], preferred_element_type=f32
                )
                total = part if total is None else total + part
            gu[n] = total
            return carry

        lax.fori_loop(first, last, tile, 0)

    def activate(k):
        for i in range(hid_tiles):
            m = hid_tiles + i
            gate = gu[i // 2, :, (i % 2) * lanes : (i % 2 + 1) * lanes]
            up = gu[m // 2, :, (m % 2) * lanes : (m % 2 + 1) * lanes]
            hid[k, :, i * lanes : (i + 1) * lanes] = (gate / (1.0 + jnp.exp(-gate)) * up).astype(bf16)

    r_p = [
        [
            remote(ps.at[i, k], pr.at[i, k], r_send.at[i, k], r_recv.at[i, k], {"tp": near})
            for k in range(4)
        ]
        for i in range(2)
    ]
    r_x = [
        remote(xs.at[k], xr.at[k], r_send.at[2, k], r_recv.at[2, k], {"tp": across}) for k in range(4)
    ]
    r_z = [
        remote(zs.at[k], zr.at[k], z_send.at[k], z_recv.at[k], {"ep": peers[k]}) for k in range(4)
    ]

    def project(k):
        for i, q in enumerate((diagonal, across, near, t)):
            part = jnp.dot(hid[k], wd[q], preferred_element_type=f32)
            if i % 2 == 0:
                ps[i // 2, k] = part.astype(bf16)
                r_p[i // 2][k].start()
            else:
                keep[i // 2, k] = part

    def send_x(k):
        r_p[0][k].wait_recv()
        xs[k] = (keep[0, k] + pr[0, k].astype(f32)).astype(bf16)
        r_x[k].start()

    def send_z(k):
        r_p[1][k].wait_recv()
        r_x[k].wait_recv()
        zs[k] = (keep[1, k] + pr[1, k].astype(f32) + xr[k].astype(f32)).astype(bf16)
        if k > 0:
            r_z[k].start()

    half = hid_tiles // 2
    for c in loads:
        c.wait()
    expand(0, 0, half)
    from_z(1)
    expand(0, half, hid_tiles)
    activate(0)
    from_z(2)
    from_x(1)
    for c in load_d:
        c.wait()
    project(0)
    from_near(1)
    expand(1, 0, half)
    from_x(2)
    from_z(3)
    expand(1, half, hid_tiles)
    activate(1)
    project(1)
    send_x(1)
    from_near(2)
    expand(2, 0, half)
    from_x(3)
    send_x(0)
    expand(2, half, hid_tiles)
    activate(2)
    project(2)
    from_near(3)
    expand(3, 0, half)
    send_x(2)
    expand(3, half, hid_tiles)
    activate(3)
    send_z(1)
    send_z(0)
    send_z(2)
    project(3)
    send_x(3)
    m_p[0].wait_recv()
    xs_m[...] = (keep_m[0] + pr_m[0].astype(f32)).astype(bf16)
    m_x = remote(xs_m, xr_m, m_send.at[2], m_recv.at[2], {"tp": across})
    m_x.start()
    send_z(3)
    m_p[1].wait_recv()
    mix_sum = keep_m[1] + pr_m[1].astype(f32)

    def share(k):
        block = zs[0] if k == 0 else zr[k]
        return shares[k] * jnp.dot(places[k], block, preferred_element_type=f32)

    result = share(0)
    r_z[1].wait_recv()
    result = result + share(1)
    m_x.wait_recv()
    mix_out[...] = (mix_sum + xr_m[...].astype(f32)).astype(bf16)
    for k in (2, 3):
        r_z[k].wait_recv()
        result = result + share(k)
    exp_out[...] = result.astype(bf16)

    @pl.when(z < 3)
    def _():
        halo_copy.wait_send()

    for c in d_z + d_x + d_p + d_q + r_p[0] + r_p[1] + r_x + r_z[1:] + m_p + [m_x]:
        c.wait_send()


def fused(
    mix_input,
    group_weight,
    pool_gain,
    branch_weight,
    exp_input,
    norm_gain,
    routes,
    route_weights,
    gate_weight,
    up_weight,
    down_weight,
):
    tokens, width = exp_input.shape
    rows_mix, channels = mix_input.shape
    hidden = gate_weight.shape[2]
    quarter = width // 4
    cap = 3 * tokens // 4
    hid_tiles = hidden // lanes
    vmem = pl.BlockSpec(memory_space=pltpu.VMEM)
    anywhere = pl.BlockSpec(memory_space=pl.ANY)
    dma = pltpu.SemaphoreType.DMA
    return pl.pallas_call(
        fused_kernel,
        out_shape=(
            pltpu.VMEM((rows_mix, quarter), bf16),
            pltpu.VMEM((tokens, quarter), bf16),
        ),
        in_specs=[vmem] * 6 + [anywhere] * 5,
        out_specs=(vmem, vmem),
        scratch_shapes=[
            pltpu.VMEM((hid_tiles, width, 2 * lanes), bf16),
            pltpu.VMEM((4, hidden, quarter), bf16),
            pltpu.VMEM((4, channels, quarter), bf16),
            pltpu.VMEM((channels // lanes, lanes, lanes), bf16),
            pltpu.VMEM((4, tokens, quarter), bf16),
            pltpu.VMEM((4, cap, quarter), bf16),
            pltpu.VMEM((4, 4, cap, quarter), bf16),
            pltpu.VMEM((hid_tiles, cap, 2 * lanes), f32),
            pltpu.VMEM((4, cap, hidden), bf16),
            pltpu.VMEM((16, channels), bf16),
            pltpu.VMEM((rows_mix, channels), bf16),
            pltpu.VMEM((2, rows_mix, quarter), f32),
            pltpu.VMEM((2, rows_mix, quarter), bf16),
            pltpu.VMEM((2, rows_mix, quarter), bf16),
            pltpu.VMEM((rows_mix, quarter), bf16),
            pltpu.VMEM((rows_mix, quarter), bf16),
            pltpu.VMEM((2, 4, cap, quarter), f32),
            pltpu.VMEM((2, 4, cap, quarter), bf16),
            pltpu.VMEM((2, 4, cap, quarter), bf16),
            pltpu.VMEM((4, cap, quarter), bf16),
            pltpu.VMEM((4, cap, quarter), bf16),
            pltpu.VMEM((4, cap, quarter), bf16),
            pltpu.VMEM((4, cap, quarter), bf16),
            dma((2 * hid_tiles + 9,)),
            dma((3, 4)),
            dma((3, 4)),
            dma((3, 4)),
            dma((3, 4)),
            dma((4,)),
            dma((4,)),
            dma((3,)),
            dma((3,)),
            dma((2,)),
        ],
        compiler_params=pltpu.CompilerParams(
            collective_id=0, has_side_effects=True, vmem_limit_bytes=56 << 20
        ),
    )(
        exp_input,
        norm_gain.reshape(1, -1),
        routes.T,
        route_weights.T,
        mix_input,
        pool_gain.reshape(1, -1),
        group_weight,
        branch_weight,
        gate_weight,
        up_weight,
        down_weight,
    )


def fits(mesh, args):
    mix, group, _, _, tok, _, routes, _, gate, _, _ = args
    ep, tp, grp = (mesh.shape[k] for k in ("ep", "tp", "grp"))
    if ep != 4 or tp != 4 or routes.shape[1] != 2 or gate.shape[0] != ep:
        return False
    rows, channels = mix.shape[0] // (grp * ep), mix.shape[1] // tp
    tokens, quarter = tok.shape[0] // (grp * ep), tok.shape[1] // tp
    return (
        group.shape[1] == lanes
        and channels % (4 * lanes) == 0
        and channels == quarter
        and rows % 16 == 0
        and tokens % 64 == 0
        and gate.shape[2] % (tp * lanes) == 0
        and gate.shape[1] * gate.shape[2] <= 1 << 23
        and rows <= 512
        and tokens <= 256
    )


def solution(mesh):
    def run(*args):
        body = fused if fits(mesh, args) else on_device
        return jax.shard_map(
            body,
            mesh=mesh,
            in_specs=(
                P(("grp", "ep"), "tp"),
                P(),
                P(),
                P("tp", None),
                P(("grp", "ep"), None),
                P(),
                P(("grp", "ep"), None),
                P(("grp", "ep"), None),
                P("ep", None, "tp"),
                P("ep", None, "tp"),
                P("ep", "tp", None),
            ),
            out_specs=(P(("grp", "ep"), "tp"), P(("grp", "ep"), "tp")),
            check_vma=False,
        )(*args)

    return run
```

profile of v0, /device:TPU:0, one launch (start us, length us, event | category | flops | bytes accessed | tf_op | source)
XLA Modules:
  0.0 45.0 jit_solution(6771762178862747608)
XLA Ops:
  0.6 43.0 %shard_map.122 = (bf16[256,512]{1,0:T(8,128)(2,1)S(1)}, bf16[128,512]{1,0:T(8,128)(2,1)S(1)}) custom-call(bf16[128,2048]{1,0:T(8,128)(2,1)} %x_ref.1, f32[1,2048]{1,0:T(1,128)} %bitcast.4, s32[2,128]{1,0:T(2,128)} %bitcast.6, f32[2,128]{1,0:T(2,128)} %bitcast.7, bf16[256,512]{1,0:T(8,128)(2,1)} %mix_ref.1, f32[1,2048]{1,0:T(1,128)} %bitcast.5, ...), custom_call_target="tpu_custom_call" | custom-call | tf_op jit(solution)/shard_map/pallas_call | solution.py:510
  43.7 0.7 %copy.15 = bf16[256,512]{1,0:T(8,128)(2,1)} copy(bf16[256,512]{1,0:T(8,128)(2,1)S(1)} %get-tuple-element.2) | data formatting | bytes 524288
  44.4 0.7 %copy.16 = bf16[128,512]{1,0:T(8,128)(2,1)} copy(bf16[128,512]{1,0:T(8,128)(2,1)S(1)} %get-tuple-element.3) | data formatting | bytes 262144
where the time goes:
time: 45.2 us; the launch traced here: 45 us
  Pallas kernels  43 us (95%)
  local copies, waits for them, and re-layouts  1.36 us (3%)
  between operations  0.64 us (1%)
    pallas_call x1, Pallas kernels, fused(): pl.pallas_call(fused_kernel, out_shape=(pltpu.VMEM((rows_mix, quarter), b...  43 us
    unnamed x2, local copies, waits for them, and re-layouts  1.36 us

commit v1 on v0

--- a/solution.py
+++ b/solution.py
@@ -146,12 +146,12 @@
 
 
 def fused_kernel(
-    x_ref,
-    norm_ref,
-    routes_ref,
-    weights_ref,
-    mix_ref,
-    gain_ref,
+    x_hbm,
+    norm_hbm,
+    routes_hbm,
+    weights_hbm,
+    mix_hbm,
+    gain_hbm,
     groups_hbm,
     branch_hbm,
     gate_hbm,
@@ -159,6 +159,12 @@
     down_hbm,
     mix_out,
     exp_out,
+    x_ref,
+    norm_ref,
+    routes_ref,
+    weights_ref,
+    mix_ref,
+    gain_ref,
     wgu,
     wd,
     wb,
@@ -183,8 +189,13 @@
     zs,
     zr,
     w_sem,
+    i_sem,
     d_send,
     d_recv,
+    f_send,
+    f_recv,
+    p_send,
+    p_recv,
     r_send,
     r_recv,
     z_send,
@@ -198,14 +209,40 @@
     near = t + 1 - 2 * (t % 2)
     across = (t + 2) % 4
     diagonal = (near + 2) % 4
+    inner = ((z + 1) // 2) % 2
     peers = [z, z + 1 - 2 * (z % 2), 3 - z, (z + 2) % 4]
+    landing = 3 - inner
+    homes = [0, 1, 3 - inner, 2 + inner]
+    home_of = [
+        z,
+        peers[1],
+        inner * peers[2] + (1 - inner) * peers[3],
+        inner * peers[3] + (1 - inner) * peers[2],
+    ]
     tokens, width = x_ref.shape
     quarter = width // 4
     cap = xg.shape[2]
+    piece = cap // 2
     hid_tiles = gate_hbm.shape[2] // lanes
     rows_mix, channels = mix_ref.shape
+    half_mix = rows_mix // 2
     group_count = channels // lanes
 
+    barrier = pltpu.get_barrier_semaphore()
+    for k in (1, 2, 3):
+        pl.semaphore_signal(barrier, inc=1, device_id={"ep": peers[k]}, device_id_type=MESH)
+    for k in (near, across):
+        pl.semaphore_signal(barrier, inc=1, device_id={"tp": k}, device_id_type=MESH)
+
+    pairs = (
+        (x_hbm, x_ref),
+        (norm_hbm, norm_ref),
+        (routes_hbm, routes_ref),
+        (weights_hbm, weights_ref),
+        (mix_hbm, mix_ref),
+        (gain_hbm, gain_ref),
+    )
+    load_i = [pltpu.make_async_copy(src, dst, i_sem.at[i]) for i, (src, dst) in enumerate(pairs)]
     loads = []
     for i in range(2 * hid_tiles):
         src = gate_hbm if i < hid_tiles else up_hbm
@@ -227,21 +264,18 @@
         for k in range(4)
     ]
     load_g = pltpu.make_async_copy(groups_hbm.at[pl.ds(t * group_count, group_count)], gw, w_sem.at[n0 + 8])
-    load_g.start()
-    for c in load_b + loads + load_d:
+    for c in load_i:
         c.start()
-
-    barrier = pltpu.get_barrier_semaphore()
-    for k in (1, 2, 3):
-        pl.semaphore_signal(barrier, inc=1, device_id={"ep": peers[k]}, device_id_type=MESH)
-    for k in (near, across):
-        pl.semaphore_signal(barrier, inc=1, device_id={"tp": k}, device_id_type=MESH)
 
     def remote(src, dst, send, recv, who):
         return pltpu.make_async_remote_copy(
             src_ref=src, dst_ref=dst, send_sem=send, recv_sem=recv, device_id=who, device_id_type=MESH
         )
 
+    for c in load_i[:4]:
+        c.wait()
+    for c in [load_g] + load_b + loads + load_d:
+        c.start()
     floated = x_ref[...].astype(f32)
     scale = lax.rsqrt(jnp.mean(floated * floated, axis=1, keepdims=True) + epsilon)
     xn_val = (floated * scale * norm_ref[...]).astype(bf16)
@@ -284,9 +318,33 @@
         ).astype(bf16)
 
     own_cols = xn[t]
-    for k in (1, 2, 3):
+    sb[0] = gathered(1, own_cols)
+    for k in (2, 3):
         sb[k] = gathered(k, own_cols)
+    sb[1] = gathered(1, xn[across])
+    for c in load_i[4:]:
+        c.wait()
     pl.semaphore_wait(barrier, 5)
+
+    def d_z(j, p):
+        rows = pl.ds(p * piece, piece)
+        q = across if j == 1 else t
+        slot = 1 if j < 2 else landing
+        at = j if j < 2 else landing
+        return remote(
+            sb.at[j, rows],
+            xg.at[q, slot, rows],
+            d_send.at[j, p],
+            d_recv.at[at, p],
+            {"ep": peers[max(j, 1)]},
+        )
+
+    sent = []
+
+    def launch(c):
+        c.start()
+        sent.append(c)
+
     halo_copy = remote(
         mix_ref.at[pl.ds(rows_mix - 16, 16), :], halo, h_sem.at[0], h_sem.at[1], {"ep": (z + 1) % 4}
     )
@@ -295,76 +353,96 @@
     def _():
         halo_copy.start()
 
-    d_z = []
-    for k in (1, 2, 3):
-        c = remote(sb.at[k], xg.at[t, k], d_send.at[k - 1, 0], d_recv.at[k - 1, 0], {"ep": peers[k]})
-        c.start()
-        d_z.append(c)
+    for j in range(4):
+        for p in range(2):
+            launch(d_z(j, p))
     for q in range(4):
         xg[q, 0] = gathered(0, xn[q])
 
-    @pl.when(z == 0)
-    def _():
-        halo[...] = jnp.zeros_like(halo)
-
-    @pl.when(z > 0)
-    def _():
-        halo_copy.wait_recv()
-
-    load_g.wait()
-    position = z * rows_mix + lax.broadcasted_iota(jnp.int32, (rows_mix, lanes), 0)
-    for g in range(group_count):
-        cols = slice(g * lanes, (g + 1) * lanes)
-        current = mix_ref[:, cols].astype(f32)
-        total = jnp.concatenate([halo[:, cols].astype(f32), current], axis=0)
-        level = g % 4
-        for step in range(level + 1):
-            total = total + pltpu.roll(total, 1 << step, 0)
-        counted = jnp.minimum(position + 1, windows[level]).astype(f32)
-        deviation = (total[16:] / counted - current).astype(bf16)
-        grouped = jnp.dot(deviation, gw[g], preferred_element_type=f32)
-        gain = gain_ref[:, pl.ds(pl.multiple_of(t * channels + g * lanes, lanes), lanes)]
-        pooled[:, cols] = (grouped * gain).astype(bf16)
-    for c in load_b:
-        c.wait()
-
-    m_p = []
-    for i, q in enumerate((diagonal, near)):
-        ps_m[i] = jnp.dot(pooled[...], wb[q], preferred_element_type=f32).astype(bf16)
-        c = remote(ps_m.at[i], pr_m.at[i], m_send.at[i], m_recv.at[i], {"tp": near})
-        c.start()
-        m_p.append(c)
-    for i, q in enumerate((across, t)):
-        keep_m[i] = jnp.dot(pooled[...], wb[q], preferred_element_type=f32)
-
-    d_x = [
-        remote(xg.at[t, k], xg.at[t, k], d_send.at[k - 1, 1], d_recv.at[k - 1, 1], {"tp": across})
-        for k in (1, 2, 3)
-    ]
-    d_p = [
-        remote(xg.at[t, k], xg.at[t, k], d_send.at[k - 1, 2], d_recv.at[k - 1, 2], {"tp": near})
-        for k in (1, 2, 3)
-    ]
-    d_q = [
-        remote(xg.at[across, k], xg.at[across, k], d_send.at[k - 1, 3], d_recv.at[k - 1, 3], {"tp": near})
-        for k in (1, 2, 3)
-    ]
+    def arrival(at, q, slot, p):
+        rows = pl.ds(p * piece, piece)
+        return remote(
+            sb.at[0, rows], xg.at[q, slot, rows], d_send.at[0, p], d_recv.at[at, p], {"ep": peers[1]}
+        )
+
+    def forward(i, q, slot, p):
+        rows = pl.ds(p * piece, piece)
+        block = xg.at[q, slot, rows]
+        return remote(
+            block, block, f_send.at[i, slot, p], f_recv.at[i, slot, p], {"tp": across if i == 0 else near}
+        )
 
     def from_z(k):
-        d_z[k - 1].wait_recv()
-        d_x[k - 1].start()
-        d_p[k - 1].start()
+        if k == 1:
+            for p in range(2):
+                arrival(0, t, 1, p).wait_recv()
+                launch(forward(1, t, 1, p))
+            for p in range(2):
+                arrival(1, across, 1, p).wait_recv()
+                launch(forward(2, across, 1, p))
+            return
+        for p in range(2):
+            arrival(k, t, k, p).wait_recv()
+            launch(forward(0, t, k, p))
+            launch(forward(1, t, k, p))
 
     def from_x(k):
-        d_x[k - 1].wait_recv()
-        d_q[k - 1].start()
+        for p in range(2):
+            forward(0, across, k, p).wait_recv()
+            launch(forward(2, across, k, p))
 
     def from_near(k):
-        d_p[k - 1].wait_recv()
-        d_q[k - 1].wait_recv()
+        for p in range(2):
+            forward(1, near, k, p).wait_recv()
+            forward(2, diagonal, k, p).wait_recv()
+
+    def mix_half(h):
+        rows = slice(h * half_mix, (h + 1) * half_mix)
+        position = z * rows_mix + h * half_mix + lax.broadcasted_iota(jnp.int32, (half_mix, lanes), 0)
+        for g in range(group_count):
+            cols = slice(g * lanes, (g + 1) * lanes)
+            current = mix_ref[rows, cols].astype(f32)
+            if h == 0:
+                past = halo[:, cols].astype(f32)
+            else:
+                past = mix_ref[h * half_mix - 16 : h * half_mix, cols].astype(f32)
+            total = jnp.concatenate([past, current], axis=0)
+            level = g % 4
+            for step in range(level + 1):
+                total = total + pltpu.roll(total, 1 << step, 0)
+            counted = jnp.minimum(position + 1, windows[level]).astype(f32)
+            deviation = (total[16:] / counted - current).astype(bf16)
+            grouped = jnp.dot(deviation, gw[g], preferred_element_type=f32)
+            gain = gain_ref[:, pl.ds(pl.multiple_of(t * channels + g * lanes, lanes), lanes)]
+            pooled[rows, cols] = (grouped * gain).astype(bf16)
+        for i, q in enumerate((diagonal, near)):
+            ps_m[h, i] = jnp.dot(pooled[rows], wb[q], preferred_element_type=f32).astype(bf16)
+            launch(m_p(h, i))
+        for i, q in enumerate((across, t)):
+            keep_m[h, i] = jnp.dot(pooled[rows], wb[q], preferred_element_type=f32)
+
+    def m_p(h, i):
+        return remote(ps_m.at[h, i], pr_m.at[h, i], m_send.at[h, i], m_recv.at[h, i], {"tp": near})
+
+    def m_x(h):
+        return remote(xs_m.at[h], xr_m.at[h], m_send.at[h, 2], m_recv.at[h, 2], {"tp": across})
+
+    def send_mix(h):
+        m_p(h, 0).wait_recv()
+        xs_m[h] = (keep_m[h, 0] + pr_m[h, 0].astype(f32)).astype(bf16)
+        launch(m_x(h))
+
+    def finish_mix(h):
+        m_p(h, 1).wait_recv()
+        m_x(h).wait_recv()
+        total = keep_m[h, 1] + pr_m[h, 1].astype(f32) + xr_m[h].astype(f32)
+        mix_out[h * half_mix : (h + 1) * half_mix] = total.astype(bf16)
 
     def expand(k, first, last):
-        def tile(n, carry):
+        for n in range(first, last):
+            if k == 0:
+                loads[2 * n].wait()
+                loads[2 * n + 1].wait()
             total = None
             for q in range(4):
                 part = jnp.dot(
@@ -372,9 +450,6 @@
                 )
                 total = part if total is None else total + part
             gu[n] = total
-            return carry
-
-        lax.fori_loop(first, last, tile, 0)
 
     def activate(k):
         for i in range(hid_tiles):
@@ -383,97 +458,113 @@
             up = gu[m // 2, :, (m % 2) * lanes : (m % 2 + 1) * lanes]
             hid[k, :, i * lanes : (i + 1) * lanes] = (gate / (1.0 + jnp.exp(-gate)) * up).astype(bf16)
 
-    r_p = [
-        [
-            remote(ps.at[i, k], pr.at[i, k], r_send.at[i, k], r_recv.at[i, k], {"tp": near})
-            for k in range(4)
-        ]
-        for i in range(2)
-    ]
-    r_x = [
-        remote(xs.at[k], xr.at[k], r_send.at[2, k], r_recv.at[2, k], {"tp": across}) for k in range(4)
-    ]
-    r_z = [
-        remote(zs.at[k], zr.at[k], z_send.at[k], z_recv.at[k], {"ep": peers[k]}) for k in range(4)
-    ]
+    def r_p(i, k):
+        return remote(ps.at[i, k], pr.at[i, k], p_send.at[i, k], p_recv.at[i, k], {"tp": near})
+
+    def r_x(k, p):
+        rows = pl.ds(p * piece, piece)
+        return remote(xs.at[k, rows], xr.at[k, rows], r_send.at[k, p], r_recv.at[k, p], {"tp": across})
+
+    def r_z(k, p):
+        rows = pl.ds(p * piece, piece)
+        return remote(
+            zs.at[k, rows],
+            zr.at[homes[k], rows],
+            z_send.at[k, p],
+            z_recv.at[homes[k], p],
+            {"ep": home_of[k]},
+        )
 
     def project(k):
         for i, q in enumerate((diagonal, across, near, t)):
             part = jnp.dot(hid[k], wd[q], preferred_element_type=f32)
             if i % 2 == 0:
                 ps[i // 2, k] = part.astype(bf16)
-                r_p[i // 2][k].start()
+                launch(r_p(i // 2, k))
             else:
                 keep[i // 2, k] = part
 
     def send_x(k):
-        r_p[0][k].wait_recv()
-        xs[k] = (keep[0, k] + pr[0, k].astype(f32)).astype(bf16)
-        r_x[k].start()
+        r_p(0, k).wait_recv()
+        for p in range(2):
+            rows = slice(p * piece, (p + 1) * piece)
+            xs[k, rows] = (keep[0, k, rows] + pr[0, k, rows].astype(f32)).astype(bf16)
+            launch(r_x(k, p))
 
     def send_z(k):
-        r_p[1][k].wait_recv()
-        r_x[k].wait_recv()
-        zs[k] = (keep[1, k] + pr[1, k].astype(f32) + xr[k].astype(f32)).astype(bf16)
-        if k > 0:
-            r_z[k].start()
+        r_p(1, k).wait_recv()
+        for p in range(2):
+            rows = slice(p * piece, (p + 1) * piece)
+            r_x(k, p).wait_recv()
+            zs[k, rows] = (keep[1, k, rows] + pr[1, k, rows].astype(f32) + xr[k, rows].astype(f32)).astype(bf16)
+            if k > 0:
+                launch(r_z(k, p))
+
+    def share(k):
+        block = zs[0] if k == 0 else zr[k]
+        return shares[k] * jnp.dot(places[k], block, preferred_element_type=f32)
+
+    def returned(k):
+        for p in range(2):
+            rows = pl.ds(p * piece, piece)
+            remote(
+                zs.at[k, rows], zr.at[k, rows], z_send.at[k, p], z_recv.at[k, p], {"ep": peers[k]}
+            ).wait_recv()
 
     half = hid_tiles // 2
-    for c in loads:
+    load_g.wait()
+    for c in load_b:
         c.wait()
-    expand(0, 0, half)
-    from_z(1)
-    expand(0, half, hid_tiles)
+    mix_half(1)
+    expand(0, 0, hid_tiles)
+    send_mix(1)
     activate(0)
-    from_z(2)
-    from_x(1)
+
+    @pl.when(z == 0)
+    def _():
+        halo[...] = jnp.zeros_like(halo)
+
+    @pl.when(z > 0)
+    def _():
+        halo_copy.wait_recv()
+
+    mix_half(0)
     for c in load_d:
         c.wait()
     project(0)
+    from_z(2)
+    send_x(0)
+    from_z(1)
     from_near(1)
-    expand(1, 0, half)
+    expand(1, 0, hid_tiles)
+    activate(1)
+    project(1)
     from_x(2)
     from_z(3)
-    expand(1, half, hid_tiles)
-    activate(1)
-    project(1)
     send_x(1)
     from_near(2)
-    expand(2, 0, half)
-    from_x(3)
-    send_x(0)
-    expand(2, half, hid_tiles)
+    expand(2, 0, hid_tiles)
     activate(2)
     project(2)
-    from_near(3)
-    expand(3, 0, half)
+    from_x(3)
     send_x(2)
-    expand(3, half, hid_tiles)
-    activate(3)
     send_z(1)
     send_z(0)
+    from_near(3)
+    expand(3, 0, hid_tiles)
+    activate(3)
+    project(3)
     send_z(2)
-    project(3)
     send_x(3)
-    m_p[0].wait_recv()
-    xs_m[...] = (keep_m[0] + pr_m[0].astype(f32)).astype(bf16)
-    m_x = remote(xs_m, xr_m, m_send.at[2], m_recv.at[2], {"tp": across})
-    m_x.start()
+    send_mix(0)
+    finish_mix(1)
+    result = share(0)
+    returned(1)
+    result = result + share(1)
     send_z(3)
-    m_p[1].wait_recv()
-    mix_sum = keep_m[1] + pr_m[1].astype(f32)
-
-    def share(k):
-        block = zs[0] if k == 0 else zr[k]
-        return shares[k] * jnp.dot(places[k], block, preferred_element_type=f32)
-
-    result = share(0)
-    r_z[1].wait_recv()
-    result = result + share(1)
-    m_x.wait_recv()
-    mix_out[...] = (mix_sum + xr_m[...].astype(f32)).astype(bf16)
+    finish_mix(0)
     for k in (2, 3):
-        r_z[k].wait_recv()
+        returned(k)
         result = result + share(k)
     exp_out[...] = result.astype(bf16)
 
@@ -481,7 +572,7 @@
     def _():
         halo_copy.wait_send()
 
-    for c in d_z + d_x + d_p + d_q + r_p[0] + r_p[1] + r_x + r_z[1:] + m_p + [m_x]:
+    for c in sent:
         c.wait_send()
 
 
@@ -504,6 +595,7 @@
     quarter = width // 4
     cap = 3 * tokens // 4
     hid_tiles = hidden // lanes
+    half_mix = rows_mix // 2
     vmem = pl.BlockSpec(memory_space=pltpu.VMEM)
     anywhere = pl.BlockSpec(memory_space=pl.ANY)
     dma = pltpu.SemaphoreType.DMA
@@ -513,9 +605,15 @@
             pltpu.VMEM((rows_mix, quarter), bf16),
             pltpu.VMEM((tokens, quarter), bf16),
         ),
-        in_specs=[vmem] * 6 + [anywhere] * 5,
+        in_specs=[anywhere] * 11,
         out_specs=(vmem, vmem),
         scratch_shapes=[
+            pltpu.VMEM((tokens, width), bf16),
+            pltpu.VMEM((1, width), f32),
+            pltpu.VMEM((2, tokens), jnp.int32),
+            pltpu.VMEM((2, tokens), f32),
+            pltpu.VMEM((rows_mix, channels), bf16),
+            pltpu.VMEM((1, 4 * channels), f32),
             pltpu.VMEM((hid_tiles, width, 2 * lanes), bf16),
             pltpu.VMEM((4, hidden, quarter), bf16),
             pltpu.VMEM((4, channels, quarter), bf16),
@@ -527,11 +625,11 @@
             pltpu.VMEM((4, cap, hidden), bf16),
             pltpu.VMEM((16, channels), bf16),
             pltpu.VMEM((rows_mix, channels), bf16),
-            pltpu.VMEM((2, rows_mix, quarter), f32),
-            pltpu.VMEM((2, rows_mix, quarter), bf16),
-            pltpu.VMEM((2, rows_mix, quarter), bf16),
-            pltpu.VMEM((rows_mix, quarter), bf16),
-            pltpu.VMEM((rows_mix, quarter), bf16),
+            pltpu.VMEM((2, 2, half_mix, quarter), f32),
+            pltpu.VMEM((2, 2, half_mix, quarter), bf16),
+            pltpu.VMEM((2, 2, half_mix, quarter), bf16),
+            pltpu.VMEM((2, half_mix, quarter), bf16),
+            pltpu.VMEM((2, half_mix, quarter), bf16),
             pltpu.VMEM((2, 4, cap, quarter), f32),
             pltpu.VMEM((2, 4, cap, quarter), bf16),
             pltpu.VMEM((2, 4, cap, quarter), bf16),
@@ -540,14 +638,19 @@
             pltpu.VMEM((4, cap, quarter), bf16),
             pltpu.VMEM((4, cap, quarter), bf16),
             dma((2 * hid_tiles + 9,)),
-            dma((3, 4)),
-            dma((3, 4)),
-            dma((3, 4)),
-            dma((3, 4)),
-            dma((4,)),
-            dma((4,)),
-            dma((3,)),
-            dma((3,)),
+            dma((6,)),
+            dma((4, 2)),
+            dma((4, 2)),
+            dma((3, 4, 2)),
+            dma((3, 4, 2)),
+            dma((2, 4)),
+            dma((2, 4)),
+            dma((4, 2)),
+            dma((4, 2)),
+            dma((4, 2)),
+            dma((4, 2)),
+            dma((2, 3)),
+            dma((2, 3)),
             dma((2,)),
         ],
         compiler_params=pltpu.CompilerParams(
@@ -579,7 +682,7 @@
         group.shape[1] == lanes
         and channels % (4 * lanes) == 0
         and channels == quarter
-        and rows % 16 == 0
+        and rows % 32 == 0
         and tokens % 64 == 0
         and gate.shape[2] % (tp * lanes) == 0
         and gate.shape[1] * gate.shape[2] <= 1 << 23

time: 45.2 us -> 40.2 us (0.89)
  Pallas kernels: 43 us -> 38 us
    pallas_call x1, Pallas kernels: 43 us -> 38 us  [fused(): pl.pallas_call(fused_kernel, out_shape=(pltpu.VMEM((rows_mix, quarter), b...]
where the time goes in v1:
time: 40.2 us; the launch traced here: 40 us
  Pallas kernels  38 us (95%)
  local copies, waits for them, and re-layouts  1.36 us (3%)
  between operations  0.64 us (2%)
    pallas_call x1, Pallas kernels, fused(): pl.pallas_call(fused_kernel, out_shape=(pltpu.VMEM((rows_mix, quarter), b...  38 us
    unnamed x2, local copies, waits for them, and re-layouts  1.36 us

profile of v1, /device:TPU:0, one launch (start us, length us, event | category | flops | bytes accessed | tf_op | source)
XLA Modules:
  0.0 40.0 jit_solution(15597267304002780967)
XLA Ops:
  0.6 38.0 %shard_map.122 = (bf16[256,512]{1,0:T(8,128)(2,1)S(1)}, bf16[128,512]{1,0:T(8,128)(2,1)S(1)}) custom-call(bf16[128,2048]{1,0:T(8,128)(2,1)} %x_hbm.1, f32[1,2048]{1,0:T(1,128)} %bitcast.4, s32[2,128]{1,0:T(2,128)} %bitcast.6, f32[2,128]{1,0:T(2,128)} %bitcast.7, bf16[256,512]{1,0:T(8,128)(2,1)} %mix_hbm.1, f32[1,2048]{1,0:T(1,128)} %bitcast.5, ...), custom_call_target="tpu_custom_call" | custom-call | tf_op jit(solution)/shard_map/pallas_call | solution.py:602
  38.7 0.7 %copy.15 = bf16[256,512]{1,0:T(8,128)(2,1)} copy(bf16[256,512]{1,0:T(8,128)(2,1)S(1)} %get-tuple-element.2) | data formatting | bytes 524288
  39.4 0.7 %copy.16 = bf16[128,512]{1,0:T(8,128)(2,1)} copy(bf16[128,512]{1,0:T(8,128)(2,1)S(1)} %get-tuple-element.3) | data formatting | bytes 262144

commit v2 on v1

--- a/solution.py
+++ b/solution.py
@@ -212,12 +212,13 @@
     inner = ((z + 1) // 2) % 2
     peers = [z, z + 1 - 2 * (z % 2), 3 - z, (z + 2) % 4]
     landing = 3 - inner
-    homes = [0, 1, 3 - inner, 2 + inner]
+    slots = [0, 3 - 2 * inner, 2 + inner, 1 + inner]
+    homes = [0, 2 - inner, 3, 1 + inner]
     home_of = [
         z,
-        peers[1],
-        inner * peers[2] + (1 - inner) * peers[3],
-        inner * peers[3] + (1 - inner) * peers[2],
+        inner * peers[1] + (1 - inner) * peers[2],
+        peers[3],
+        inner * peers[2] + (1 - inner) * peers[1],
     ]
     tokens, width = x_ref.shape
     quarter = width // 4
@@ -317,6 +318,12 @@
             places[k], block, (((0,), (0,)), ((), ())), preferred_element_type=f32
         ).astype(bf16)
 
+    def if_inner(step, k):
+        pl.when(inner == 1)(lambda: step(k))
+
+    def if_outer(step, k):
+        pl.when(inner == 0)(lambda: step(k))
+
     own_cols = xn[t]
     sb[0] = gathered(1, own_cols)
     for k in (2, 3):
@@ -339,12 +346,6 @@
             {"ep": peers[max(j, 1)]},
         )
 
-    sent = []
-
-    def launch(c):
-        c.start()
-        sent.append(c)
-
     halo_copy = remote(
         mix_ref.at[pl.ds(rows_mix - 16, 16), :], halo, h_sem.at[0], h_sem.at[1], {"ep": (z + 1) % 4}
     )
@@ -353,9 +354,13 @@
     def _():
         halo_copy.start()
 
-    for j in range(4):
-        for p in range(2):
-            launch(d_z(j, p))
+    def send_rows(order):
+        for j in order:
+            for p in range(2):
+                d_z(j, p).start()
+
+    if_outer(send_rows, (2, 3, 0, 1))
+    if_inner(send_rows, (3, 2, 0, 1))
     for q in range(4):
         xg[q, 0] = gathered(0, xn[q])
 
@@ -376,25 +381,25 @@
         if k == 1:
             for p in range(2):
                 arrival(0, t, 1, p).wait_recv()
-                launch(forward(1, t, 1, p))
+                forward(1, t, 1, p).start()
             for p in range(2):
                 arrival(1, across, 1, p).wait_recv()
-                launch(forward(2, across, 1, p))
+                forward(2, across, 1, p).start()
             return
         for p in range(2):
             arrival(k, t, k, p).wait_recv()
-            launch(forward(0, t, k, p))
-            launch(forward(1, t, k, p))
+            forward(0, t, k, p).start()
+            forward(1, t, k, p).start()
 
     def from_x(k):
         for p in range(2):
             forward(0, across, k, p).wait_recv()
-            launch(forward(2, across, k, p))
+            forward(2, across, k, p).start()
 
     def from_near(k):
         for p in range(2):
-            forward(1, near, k, p).wait_recv()
-            forward(2, diagonal, k, p).wait_recv()
+            forward(1, near, slots[k], p).wait_recv()
+            forward(2, diagonal, slots[k], p).wait_recv()
 
     def mix_half(h):
         rows = slice(h * half_mix, (h + 1) * half_mix)
@@ -417,7 +422,7 @@
             pooled[rows, cols] = (grouped * gain).astype(bf16)
         for i, q in enumerate((diagonal, near)):
             ps_m[h, i] = jnp.dot(pooled[rows], wb[q], preferred_element_type=f32).astype(bf16)
-            launch(m_p(h, i))
+            m_p(h, i).start()
         for i, q in enumerate((across, t)):
             keep_m[h, i] = jnp.dot(pooled[rows], wb[q], preferred_element_type=f32)
 
@@ -430,7 +435,7 @@
     def send_mix(h):
         m_p(h, 0).wait_recv()
         xs_m[h] = (keep_m[h, 0] + pr_m[h, 0].astype(f32)).astype(bf16)
-        launch(m_x(h))
+        m_x(h).start()
 
     def finish_mix(h):
         m_p(h, 1).wait_recv()
@@ -446,7 +451,7 @@
             total = None
             for q in range(4):
                 part = jnp.dot(
-                    xg[q, k], wgu[n, q * quarter : (q + 1) * quarter, :], preferred_element_type=f32
+                    xg[q, slots[k]], wgu[n, q * quarter : (q + 1) * quarter, :], preferred_element_type=f32
                 )
                 total = part if total is None else total + part
             gu[n] = total
@@ -480,7 +485,7 @@
             part = jnp.dot(hid[k], wd[q], preferred_element_type=f32)
             if i % 2 == 0:
                 ps[i // 2, k] = part.astype(bf16)
-                launch(r_p(i // 2, k))
+                r_p(i // 2, k).start()
             else:
                 keep[i // 2, k] = part
 
@@ -489,7 +494,7 @@
         for p in range(2):
             rows = slice(p * piece, (p + 1) * piece)
             xs[k, rows] = (keep[0, k, rows] + pr[0, k, rows].astype(f32)).astype(bf16)
-            launch(r_x(k, p))
+            r_x(k, p).start()
 
     def send_z(k):
         r_p(1, k).wait_recv()
@@ -498,7 +503,7 @@
             r_x(k, p).wait_recv()
             zs[k, rows] = (keep[1, k, rows] + pr[1, k, rows].astype(f32) + xr[k, rows].astype(f32)).astype(bf16)
             if k > 0:
-                launch(r_z(k, p))
+                r_z(k, p).start()
 
     def share(k):
         block = zs[0] if k == 0 else zr[k]
@@ -516,9 +521,14 @@
     for c in load_b:
         c.wait()
     mix_half(1)
-    expand(0, 0, hid_tiles)
+    expand(0, 0, half)
     send_mix(1)
+    expand(0, half, hid_tiles)
     activate(0)
+    for c in load_d:
+        c.wait()
+    project(0)
+    if_outer(from_z, 3)
 
     @pl.when(z == 0)
     def _():
@@ -529,41 +539,44 @@
         halo_copy.wait_recv()
 
     mix_half(0)
-    for c in load_d:
-        c.wait()
-    project(0)
-    from_z(2)
-    send_x(0)
+    if_inner(from_z, 3)
+    if_inner(send_x, 0)
+    if_outer(from_z, 2)
+    if_outer(send_x, 0)
+    if_outer(from_x, 3)
     from_z(1)
+    if_inner(from_z, 2)
+    if_inner(from_x, 3)
     from_near(1)
     expand(1, 0, hid_tiles)
     activate(1)
+    if_outer(from_x, 2)
     project(1)
-    from_x(2)
-    from_z(3)
+    from_near(2)
+    expand(2, 0, 2)
     send_x(1)
-    from_near(2)
-    expand(2, 0, hid_tiles)
+    expand(2, 2, hid_tiles)
     activate(2)
+    if_inner(from_x, 2)
     project(2)
-    from_x(3)
+    from_near(3)
+    expand(3, 0, 2)
     send_x(2)
+    expand(3, 2, hid_tiles)
+    activate(3)
     send_z(1)
+    project(3)
+    send_x(3)
+    send_z(2)
     send_z(0)
-    from_near(3)
-    expand(3, 0, hid_tiles)
-    activate(3)
-    project(3)
-    send_z(2)
-    send_x(3)
     send_mix(0)
     finish_mix(1)
     result = share(0)
-    returned(1)
-    result = result + share(1)
     send_z(3)
+    returned(3)
+    result = result + share(3)
     finish_mix(0)
-    for k in (2, 3):
+    for k in (1, 2):
         returned(k)
         result = result + share(k)
     exp_out[...] = result.astype(bf16)
@@ -572,8 +585,33 @@
     def _():
         halo_copy.wait_send()
 
-    for c in sent:
-        c.wait_send()
+    for k in (1, 2, 3):
+        for p in range(2):
+            if k > 1:
+                forward(0, t, k, p).wait_send()
+            forward(1, t, k, p).wait_send()
+            forward(2, across, k, p).wait_send()
+            r_z(k, p).wait_send()
+    for k in range(4):
+        for p in range(2):
+            d_z(k, p).wait_send()
+            r_x(k, p).wait_send()
+            r_p(p, k).wait_send()
+    for h in range(2):
+        m_p(h, 0).wait_send()
+        m_p(h, 1).wait_send()
+        m_x(h).wait_send()
+
+
+def store_kernel(mix_ref, exp_ref, mix_hbm, exp_hbm, sem):
+    stores = [
+        pltpu.make_async_copy(mix_ref, mix_hbm, sem.at[0]),
+        pltpu.make_async_copy(exp_ref, exp_hbm, sem.at[1]),
+    ]
+    for c in stores:
+        c.start()
+    for c in stores:
+        c.wait()
 
 
 def fused(
@@ -599,7 +637,7 @@
     vmem = pl.BlockSpec(memory_space=pltpu.VMEM)
     anywhere = pl.BlockSpec(memory_space=pl.ANY)
     dma = pltpu.SemaphoreType.DMA
-    return pl.pallas_call(
+    mix_out, exp_out = pl.pallas_call(
         fused_kernel,
         out_shape=(
             pltpu.VMEM((rows_mix, quarter), bf16),
@@ -669,6 +707,19 @@
         up_weight,
         down_weight,
     )
+    return pl.pallas_call(
+        store_kernel,
+        out_shape=(
+            jax.ShapeDtypeStruct((rows_mix, quarter), bf16),
+            jax.ShapeDtypeStruct((tokens, quarter), bf16),
+        ),
+        in_specs=[vmem] * 2,
+        out_specs=(anywhere, anywhere),
+        scratch_shapes=[dma((2,))],
+    )(
+        pltpu.with_memory_space_constraint(mix_out, pltpu.VMEM),
+        pltpu.with_memory_space_constraint(exp_out, pltpu.VMEM),
+    )
 
 
 def fits(mesh, args):

time: 40.2 us -> 37.4 us (0.930)
  Pallas kernels: 38 us -> 36.6 us
  local copies, waits for them, and re-layouts: 1.36 us -> 0 us
    pallas_call x1, Pallas kernels: 38 us -> 35.9 us  [fused(): pl.pallas_call(fused_kernel, out_shape=(pltpu.VMEM((rows_mix, quarter), b...]
    unnamed x2 -> x0, local copies, waits for them, and re-layouts: 1.36 us -> none
    pallas_call x0 -> x1, Pallas kernels: none -> 0.76 us  [fused(): pl.pallas_call(store_kernel, out_shape=(jax.ShapeDtypeStruct((rows_mix, q...]
where the time goes in v2:
time: 37.4 us; the launch traced here: 37.3 us
  Pallas kernels  36.6 us (98%)
  between operations  0.64 us (2%)
    pallas_call x1, Pallas kernels, fused(): pl.pallas_call(fused_kernel, out_shape=(pltpu.VMEM((rows_mix, quarter), b...  35.9 us
    pallas_call x1, Pallas kernels, fused(): pl.pallas_call(store_kernel, out_shape=(jax.ShapeDtypeStruct((rows_mix, q...  0.76 us

profile of v2, /device:TPU:0, one launch (start us, length us, event | category | flops | bytes accessed | tf_op | source)
XLA Modules:
  0.0 37.3 jit_solution(11405048466868754499)
XLA Ops:
  0.6 35.9 %shard_map.122 = (bf16[256,512]{1,0:T(8,128)(2,1)S(1)}, bf16[128,512]{1,0:T(8,128)(2,1)S(1)}) custom-call(bf16[128,2048]{1,0:T(8,128)(2,1)} %x_hbm.1, f32[1,2048]{1,0:T(1,128)} %bitcast.4, s32[2,128]{1,0:T(2,128)} %bitcast.6, f32[2,128]{1,0:T(2,128)} %bitcast.7, bf16[256,512]{1,0:T(8,128)(2,1)} %mix_hbm.1, f32[1,2048]{1,0:T(1,128)} %bitcast.5, ...), custom_call_target="tpu_custom_call" | custom-call | tf_op jit(solution)/shard_map/pallas_call | solution.py:640
  36.5 0.8 %shard_map.123 = (bf16[256,512]{1,0:T(8,128)(2,1)}, bf16[128,512]{1,0:T(8,128)(2,1)}) custom-call(bf16[256,512]{1,0:T(8,128)(2,1)S(1)} %get-tuple-element.4.mix_ref, bf16[128,512]{1,0:T(8,128)(2,1)S(1)} %get-tuple-element.5.exp_ref), custom_call_target="tpu_custom_call" | custom-call | tf_op jit(solution)/shard_map/pallas_call | solution.py:710

commit v3 on v2

--- a/solution.py
+++ b/solution.py
@@ -212,14 +212,18 @@
     inner = ((z + 1) // 2) % 2
     peers = [z, z + 1 - 2 * (z % 2), 3 - z, (z + 2) % 4]
     landing = 3 - inner
-    slots = [0, 3 - 2 * inner, 2 + inner, 1 + inner]
-    homes = [0, 2 - inner, 3, 1 + inner]
+    slots = [0, 3, 2 - inner, 1 + inner]
+    homes = [0, 2 + inner, 3 - 2 * inner, 1 + inner]
     home_of = [
         z,
-        inner * peers[1] + (1 - inner) * peers[2],
-        peers[3],
+        inner * peers[3] + (1 - inner) * peers[2],
+        inner * peers[1] + (1 - inner) * peers[3],
         inner * peers[2] + (1 - inner) * peers[1],
     ]
+    second = inner * across + (1 - inner) * near
+    third = inner * near + (1 - inner) * across
+    early = [None, (t, near), (t, second), (t, third)]
+    late = [None, (across, diagonal), (third, diagonal), (second, diagonal)]
     tokens, width = x_ref.shape
     quarter = width // 4
     cap = xg.shape[2]
@@ -236,10 +240,10 @@
         pl.semaphore_signal(barrier, inc=1, device_id={"tp": k}, device_id_type=MESH)
 
     pairs = (
+        (routes_hbm, routes_ref),
+        (weights_hbm, weights_ref),
         (x_hbm, x_ref),
         (norm_hbm, norm_ref),
-        (routes_hbm, routes_ref),
-        (weights_hbm, weights_ref),
         (mix_hbm, mix_ref),
         (gain_hbm, gain_ref),
     )
@@ -273,15 +277,8 @@
             src_ref=src, dst_ref=dst, send_sem=send, recv_sem=recv, device_id=who, device_id_type=MESH
         )
 
-    for c in load_i[:4]:
+    for c in load_i[:2]:
         c.wait()
-    for c in [load_g] + load_b + loads + load_d:
-        c.start()
-    floated = x_ref[...].astype(f32)
-    scale = lax.rsqrt(jnp.mean(floated * floated, axis=1, keepdims=True) + epsilon)
-    xn_val = (floated * scale * norm_ref[...]).astype(bf16)
-    for k in range(4):
-        xn[k] = xn_val[:, k * quarter : (k + 1) * quarter]
     lane = lax.broadcasted_iota(jnp.int32, (tokens, lanes), 1)
     square = (tokens, tokens)
     diagonal_mask = lax.broadcasted_iota(jnp.int32, square, 0) == lax.broadcasted_iota(jnp.int32, square, 1)
@@ -313,6 +310,16 @@
             + jnp.where(r1 == peers[k], w1, 0.0)
         )
 
+    for c in load_i[2:4]:
+        c.wait()
+    for c in [load_g] + load_b + loads + load_d:
+        c.start()
+    floated = x_ref[...].astype(f32)
+    scale = lax.rsqrt(jnp.mean(floated * floated, axis=1, keepdims=True) + epsilon)
+    xn_val = (floated * scale * norm_ref[...]).astype(bf16)
+    for k in range(4):
+        xn[k] = xn_val[:, k * quarter : (k + 1) * quarter]
+
     def gathered(k, block):
         return lax.dot_general(
             places[k], block, (((0,), (0,)), ((), ())), preferred_element_type=f32
@@ -325,10 +332,8 @@
         pl.when(inner == 0)(lambda: step(k))
 
     own_cols = xn[t]
-    sb[0] = gathered(1, own_cols)
     for k in (2, 3):
         sb[k] = gathered(k, own_cols)
-    sb[1] = gathered(1, xn[across])
     for c in load_i[4:]:
         c.wait()
     pl.semaphore_wait(barrier, 5)
@@ -359,8 +364,11 @@
             for p in range(2):
                 d_z(j, p).start()
 
-    if_outer(send_rows, (2, 3, 0, 1))
-    if_inner(send_rows, (3, 2, 0, 1))
+    if_outer(send_rows, (2, 3))
+    if_inner(send_rows, (3, 2))
+    sb[0] = gathered(1, own_cols)
+    sb[1] = gathered(1, xn[across])
+    send_rows((0, 1))
     for q in range(4):
         xg[q, 0] = gathered(0, xn[q])
 
@@ -396,10 +404,13 @@
             forward(0, across, k, p).wait_recv()
             forward(2, across, k, p).start()
 
-    def from_near(k):
-        for p in range(2):
-            forward(1, near, slots[k], p).wait_recv()
-            forward(2, diagonal, slots[k], p).wait_recv()
+    def near_own(k):
+        for p in range(2):
+            forward(1, near, k, p).wait_recv()
+
+    def near_other(k):
+        for p in range(2):
+            forward(2, diagonal, k, p).wait_recv()
 
     def mix_half(h):
         rows = slice(h * half_mix, (h + 1) * half_mix)
@@ -422,9 +433,10 @@
             pooled[rows, cols] = (grouped * gain).astype(bf16)
         for i, q in enumerate((diagonal, near)):
             ps_m[h, i] = jnp.dot(pooled[rows], wb[q], preferred_element_type=f32).astype(bf16)
-            m_p(h, i).start()
         for i, q in enumerate((across, t)):
             keep_m[h, i] = jnp.dot(pooled[rows], wb[q], preferred_element_type=f32)
+        for i in range(2):
+            m_p(h, i).start()
 
     def m_p(h, i):
         return remote(ps_m.at[h, i], pr_m.at[h, i], m_send.at[h, i], m_recv.at[h, i], {"tp": near})
@@ -443,24 +455,23 @@
         total = keep_m[h, 1] + pr_m[h, 1].astype(f32) + xr_m[h].astype(f32)
         mix_out[h * half_mix : (h + 1) * half_mix] = total.astype(bf16)
 
-    def expand(k, first, last):
+    def expand(k, blocks, first, last):
         for n in range(first, last):
             if k == 0:
                 loads[2 * n].wait()
                 loads[2 * n + 1].wait()
-            total = None
-            for q in range(4):
-                part = jnp.dot(
-                    xg[q, slots[k]], wgu[n, q * quarter : (q + 1) * quarter, :], preferred_element_type=f32
-                )
+            total = None if blocks is None or blocks is early[k] else gu[k, n]
+            for q in range(4) if blocks is None else blocks:
+                rows = pl.ds(q * quarter if blocks is None else pl.multiple_of(q * quarter, quarter), quarter)
+                part = jnp.dot(xg[q, slots[k]], wgu[n, rows, :], preferred_element_type=f32)
                 total = part if total is None else total + part
-            gu[n] = total
+            gu[k, n] = total
 
     def activate(k):
         for i in range(hid_tiles):
             m = hid_tiles + i
-            gate = gu[i // 2, :, (i % 2) * lanes : (i % 2 + 1) * lanes]
-            up = gu[m // 2, :, (m % 2) * lanes : (m % 2 + 1) * lanes]
+            gate = gu[k, i // 2, :, (i % 2) * lanes : (i % 2 + 1) * lanes]
+            up = gu[k, m // 2, :, (m % 2) * lanes : (m % 2 + 1) * lanes]
             hid[k, :, i * lanes : (i + 1) * lanes] = (gate / (1.0 + jnp.exp(-gate)) * up).astype(bf16)
 
     def r_p(i, k):
@@ -481,13 +492,15 @@
         )
 
     def project(k):
-        for i, q in enumerate((diagonal, across, near, t)):
+        for i, q in enumerate((diagonal, near, across, t)):
             part = jnp.dot(hid[k], wd[q], preferred_element_type=f32)
-            if i % 2 == 0:
-                ps[i // 2, k] = part.astype(bf16)
-                r_p(i // 2, k).start()
+            if i < 2:
+                ps[i, k] = part.astype(bf16)
             else:
-                keep[i // 2, k] = part
+                keep[i - 2, k] = part
+            if i == 0:
+                r_p(0, k).start()
+        r_p(1, k).start()
 
     def send_x(k):
         r_p(0, k).wait_recv()
@@ -521,9 +534,9 @@
     for c in load_b:
         c.wait()
     mix_half(1)
-    expand(0, 0, half)
+    expand(0, None, 0, half)
     send_mix(1)
-    expand(0, half, hid_tiles)
+    expand(0, None, half, hid_tiles)
     activate(0)
     for c in load_d:
         c.wait()
@@ -540,32 +553,42 @@
 
     mix_half(0)
     if_inner(from_z, 3)
-    if_inner(send_x, 0)
+    near_own(3)
+    expand(1, early[1], 0, hid_tiles)
     if_outer(from_z, 2)
-    if_outer(send_x, 0)
     if_outer(from_x, 3)
     from_z(1)
     if_inner(from_z, 2)
     if_inner(from_x, 3)
-    from_near(1)
-    expand(1, 0, hid_tiles)
+    expand(1, late[1][:1], 0, hid_tiles)
+    send_x(0)
+    if_outer(near_own, 2)
+    expand(2, early[2], 0, hid_tiles)
+    near_other(3)
+    expand(1, late[1][1:], 0, hid_tiles)
     activate(1)
+    project(1)
     if_outer(from_x, 2)
-    project(1)
-    from_near(2)
-    expand(2, 0, 2)
+    if_inner(near_own, 2)
+    expand(3, early[3], 0, hid_tiles)
     send_x(1)
-    expand(2, 2, hid_tiles)
+    if_inner(near_own, 1)
+    if_inner(near_other, 1)
+    if_outer(near_other, 2)
+    expand(2, late[2], 0, hid_tiles)
     activate(2)
     if_inner(from_x, 2)
     project(2)
-    from_near(3)
-    expand(3, 0, 2)
+    if_outer(near_own, 1)
+    if_outer(near_other, 1)
+    if_inner(near_other, 2)
+    expand(3, late[3], 0, half)
     send_x(2)
-    expand(3, 2, hid_tiles)
+    expand(3, late[3], half, hid_tiles)
     activate(3)
-    send_z(1)
+    if_outer(send_z, 1)
     project(3)
+    if_inner(send_z, 1)
     send_x(3)
     send_z(2)
     send_z(0)
@@ -659,7 +682,7 @@
             pltpu.VMEM((4, tokens, quarter), bf16),
             pltpu.VMEM((4, cap, quarter), bf16),
             pltpu.VMEM((4, 4, cap, quarter), bf16),
-            pltpu.VMEM((hid_tiles, cap, 2 * lanes), f32),
+            pltpu.VMEM((4, hid_tiles, cap, 2 * lanes), f32),
             pltpu.VMEM((4, cap, hidden), bf16),
             pltpu.VMEM((16, channels), bf16),
             pltpu.VMEM((rows_mix, channels), bf16),

time: 37.4 us -> 35 us (0.936)
  Pallas kernels: 36.6 us -> 34.2 us
    pallas_call x1, Pallas kernels: 35.9 us -> 33.5 us  [fused(): pl.pallas_call(fused_kernel, out_shape=(pltpu.VMEM((rows_mix, quarter), b...]
where the time goes in v3:
time: 35 us; the launch traced here: 34.9 us
  Pallas kernels  34.2 us (98%)
  between operations  0.64 us (2%)
    pallas_call x1, Pallas kernels, fused(): pl.pallas_call(fused_kernel, out_shape=(pltpu.VMEM((rows_mix, quarter), b...  33.5 us
    pallas_call x1, Pallas kernels, fused(): pl.pallas_call(store_kernel, out_shape=(jax.ShapeDtypeStruct((rows_mix, q...  0.76 us

profile of v3, /device:TPU:0, one launch (start us, length us, event | category | flops | bytes accessed | tf_op | source)
XLA Modules:
  0.0 34.9 jit_solution(141552869636466881)
XLA Ops:
  0.6 33.5 %shard_map.122 = (bf16[256,512]{1,0:T(8,128)(2,1)S(1)}, bf16[128,512]{1,0:T(8,128)(2,1)S(1)}) custom-call(bf16[128,2048]{1,0:T(8,128)(2,1)} %x_hbm.1, f32[1,2048]{1,0:T(1,128)} %bitcast.4, s32[2,128]{1,0:T(2,128)} %bitcast.6, f32[2,128]{1,0:T(2,128)} %bitcast.7, bf16[256,512]{1,0:T(8,128)(2,1)} %mix_hbm.1, f32[1,2048]{1,0:T(1,128)} %bitcast.5, ...), custom_call_target="tpu_custom_call" | custom-call | tf_op jit(solution)/shard_map/pallas_call | solution.py:663
  34.1 0.8 %shard_map.123 = (bf16[256,512]{1,0:T(8,128)(2,1)}, bf16[128,512]{1,0:T(8,128)(2,1)}) custom-call(bf16[256,512]{1,0:T(8,128)(2,1)S(1)} %get-tuple-element.4.mix_ref, bf16[128,512]{1,0:T(8,128)(2,1)S(1)} %get-tuple-element.5.exp_ref), custom_call_target="tpu_custom_call" | custom-call | tf_op jit(solution)/shard_map/pallas_call | solution.py:733

commit v4 on v3

--- a/solution.py
+++ b/solution.py
@@ -140,6 +140,7 @@
 
 
 lanes = 128
+pieces = 2
 MESH = pl.DeviceIdType.MESH
 f32 = jnp.float32
 bf16 = jnp.bfloat16
@@ -190,17 +191,13 @@
     zr,
     w_sem,
     i_sem,
-    d_send,
+    s_sem,
     d_recv,
-    f_send,
     f_recv,
-    p_send,
+    g_recv,
     p_recv,
-    r_send,
     r_recv,
-    z_send,
     z_recv,
-    m_send,
     m_recv,
     h_sem,
 ):
@@ -227,7 +224,7 @@
     tokens, width = x_ref.shape
     quarter = width // 4
     cap = xg.shape[2]
-    piece = cap // 2
+    piece = cap // pieces
     hid_tiles = gate_hbm.shape[2] // lanes
     rows_mix, channels = mix_ref.shape
     half_mix = rows_mix // 2
@@ -248,6 +245,7 @@
         (gain_hbm, gain_ref),
     )
     load_i = [pltpu.make_async_copy(src, dst, i_sem.at[i]) for i, (src, dst) in enumerate(pairs)]
+    front = (hid_tiles + 1) // 2
     loads = []
     for i in range(2 * hid_tiles):
         src = gate_hbm if i < hid_tiles else up_hbm
@@ -256,19 +254,22 @@
             pltpu.make_async_copy(
                 src.at[0, :, pl.ds(at, lanes)],
                 wgu.at[i // 2, :, pl.ds((i % 2) * lanes, lanes)],
-                w_sem.at[i],
+                w_sem.at[0 if i // 2 < front else 1],
             )
         )
-    n0 = 2 * hid_tiles
     load_b = [
-        pltpu.make_async_copy(branch_hbm.at[:, pl.ds(k * quarter, quarter)], wb.at[k], w_sem.at[n0 + k])
+        pltpu.make_async_copy(branch_hbm.at[:, pl.ds(k * quarter, quarter)], wb.at[k], w_sem.at[2])
         for k in range(4)
     ]
     load_d = [
-        pltpu.make_async_copy(down_hbm.at[0, :, pl.ds(k * quarter, quarter)], wd.at[k], w_sem.at[n0 + 4 + k])
+        pltpu.make_async_copy(down_hbm.at[0, :, pl.ds(k * quarter, quarter)], wd.at[k], w_sem.at[3])
         for k in range(4)
     ]
-    load_g = pltpu.make_async_copy(groups_hbm.at[pl.ds(t * group_count, group_count)], gw, w_sem.at[n0 + 8])
+    load_g = pltpu.make_async_copy(groups_hbm.at[pl.ds(t * group_count, group_count)], gw, w_sem.at[4])
+
+    def loaded(ref, i):
+        pltpu.make_async_copy(ref, ref, w_sem.at[i]).wait()
+
     for c in load_i:
         c.start()
 
@@ -346,7 +347,7 @@
         return remote(
             sb.at[j, rows],
             xg.at[q, slot, rows],
-            d_send.at[j, p],
+            s_sem.at[0],
             d_recv.at[at, p],
             {"ep": peers[max(j, 1)]},
         )
@@ -361,7 +362,7 @@
 
     def send_rows(order):
         for j in order:
-            for p in range(2):
+            for p in range(pieces):
                 d_z(j, p).start()
 
     if_outer(send_rows, (2, 3))
@@ -375,42 +376,41 @@
     def arrival(at, q, slot, p):
         rows = pl.ds(p * piece, piece)
         return remote(
-            sb.at[0, rows], xg.at[q, slot, rows], d_send.at[0, p], d_recv.at[at, p], {"ep": peers[1]}
+            sb.at[0, rows], xg.at[q, slot, rows], s_sem.at[0], d_recv.at[at, p], {"ep": peers[1]}
         )
 
     def forward(i, q, slot, p):
         rows = pl.ds(p * piece, piece)
         block = xg.at[q, slot, rows]
-        return remote(
-            block, block, f_send.at[i, slot, p], f_recv.at[i, slot, p], {"tp": across if i == 0 else near}
-        )
+        landed = f_recv.at[slot, p] if i == 0 else g_recv.at[i - 1, slot]
+        return remote(block, block, s_sem.at[1], landed, {"tp": across if i == 0 else near})
 
     def from_z(k):
         if k == 1:
-            for p in range(2):
+            for p in range(pieces):
                 arrival(0, t, 1, p).wait_recv()
                 forward(1, t, 1, p).start()
-            for p in range(2):
+            for p in range(pieces):
                 arrival(1, across, 1, p).wait_recv()
                 forward(2, across, 1, p).start()
             return
-        for p in range(2):
+        for p in range(pieces):
             arrival(k, t, k, p).wait_recv()
             forward(0, t, k, p).start()
             forward(1, t, k, p).start()
 
     def from_x(k):
-        for p in range(2):
+        for p in range(pieces):
             forward(0, across, k, p).wait_recv()
             forward(2, across, k, p).start()
 
     def near_own(k):
-        for p in range(2):
-            forward(1, near, k, p).wait_recv()
+        block = xg.at[near, k]
+        remote(block, block, s_sem.at[1], g_recv.at[0, k], {"tp": near}).wait_recv()
 
     def near_other(k):
-        for p in range(2):
-            forward(2, diagonal, k, p).wait_recv()
+        block = xg.at[diagonal, k]
+        remote(block, block, s_sem.at[1], g_recv.at[1, k], {"tp": near}).wait_recv()
 
     def mix_half(h):
         rows = slice(h * half_mix, (h + 1) * half_mix)
@@ -439,10 +439,10 @@
             m_p(h, i).start()
 
     def m_p(h, i):
-        return remote(ps_m.at[h, i], pr_m.at[h, i], m_send.at[h, i], m_recv.at[h, i], {"tp": near})
+        return remote(ps_m.at[h, i], pr_m.at[h, i], s_sem.at[5], m_recv.at[h, i], {"tp": near})
 
     def m_x(h):
-        return remote(xs_m.at[h], xr_m.at[h], m_send.at[h, 2], m_recv.at[h, 2], {"tp": across})
+        return remote(xs_m.at[h], xr_m.at[h], s_sem.at[6], m_recv.at[h, 2], {"tp": across})
 
     def send_mix(h):
         m_p(h, 0).wait_recv()
@@ -457,9 +457,10 @@
 
     def expand(k, blocks, first, last):
         for n in range(first, last):
-            if k == 0:
-                loads[2 * n].wait()
-                loads[2 * n + 1].wait()
+            if k == 0 and n == 0:
+                loaded(wgu.at[pl.ds(0, front)], 0)
+            if k == 0 and n == front:
+                loaded(wgu.at[pl.ds(front, hid_tiles - front)], 1)
             total = None if blocks is None or blocks is early[k] else gu[k, n]
             for q in range(4) if blocks is None else blocks:
                 rows = pl.ds(q * quarter if blocks is None else pl.multiple_of(q * quarter, quarter), quarter)
@@ -467,6 +468,9 @@
                 total = part if total is None else total + part
             gu[k, n] = total
 
+    def expand_early(k):
+        expand(k, early[k], 0, hid_tiles)
+
     def activate(k):
         for i in range(hid_tiles):
             m = hid_tiles + i
@@ -475,19 +479,19 @@
             hid[k, :, i * lanes : (i + 1) * lanes] = (gate / (1.0 + jnp.exp(-gate)) * up).astype(bf16)
 
     def r_p(i, k):
-        return remote(ps.at[i, k], pr.at[i, k], p_send.at[i, k], p_recv.at[i, k], {"tp": near})
+        return remote(ps.at[i, k], pr.at[i, k], s_sem.at[2], p_recv.at[i, k], {"tp": near})
 
     def r_x(k, p):
         rows = pl.ds(p * piece, piece)
-        return remote(xs.at[k, rows], xr.at[k, rows], r_send.at[k, p], r_recv.at[k, p], {"tp": across})
+        return remote(xs.at[k, rows], xr.at[k, rows], s_sem.at[3], r_recv.at[k, p], {"tp": across})
 
     def r_z(k, p):
         rows = pl.ds(p * piece, piece)
         return remote(
             zs.at[k, rows],
             zr.at[homes[k], rows],
-            z_send.at[k, p],
-            z_recv.at[homes[k], p],
+            s_sem.at[4],
+            z_recv.at[homes[k]],
             {"ep": home_of[k]},
         )
 
@@ -504,14 +508,15 @@
 
     def send_x(k):
         r_p(0, k).wait_recv()
-        for p in range(2):
+        for p in range(pieces):
             rows = slice(p * piece, (p + 1) * piece)
             xs[k, rows] = (keep[0, k, rows] + pr[0, k, rows].astype(f32)).astype(bf16)
             r_x(k, p).start()
 
-    def send_z(k):
-        r_p(1, k).wait_recv()
-        for p in range(2):
+    def send_z(k, first=0, last=pieces):
+        if first == 0:
+            r_p(1, k).wait_recv()
+        for p in range(first, last):
             rows = slice(p * piece, (p + 1) * piece)
             r_x(k, p).wait_recv()
             zs[k, rows] = (keep[1, k, rows] + pr[1, k, rows].astype(f32) + xr[k, rows].astype(f32)).astype(bf16)
@@ -523,23 +528,20 @@
         return shares[k] * jnp.dot(places[k], block, preferred_element_type=f32)
 
     def returned(k):
-        for p in range(2):
-            rows = pl.ds(p * piece, piece)
-            remote(
-                zs.at[k, rows], zr.at[k, rows], z_send.at[k, p], z_recv.at[k, p], {"ep": peers[k]}
-            ).wait_recv()
+        remote(zs.at[k], zr.at[k], s_sem.at[4], z_recv.at[k], {"ep": peers[k]}).wait_recv()
+
+    def left(ref, i):
+        remote(ref, ref, s_sem.at[i], s_sem.at[i], {"tp": near}).wait_send()
 
     half = hid_tiles // 2
     load_g.wait()
-    for c in load_b:
-        c.wait()
+    loaded(wb, 2)
     mix_half(1)
     expand(0, None, 0, half)
     send_mix(1)
     expand(0, None, half, hid_tiles)
     activate(0)
-    for c in load_d:
-        c.wait()
+    loaded(wd, 3)
     project(0)
     if_outer(from_z, 3)
 
@@ -561,41 +563,56 @@
     if_inner(from_z, 2)
     if_inner(from_x, 3)
     expand(1, late[1][:1], 0, hid_tiles)
-    send_x(0)
     if_outer(near_own, 2)
     expand(2, early[2], 0, hid_tiles)
+    send_x(0)
     near_other(3)
     expand(1, late[1][1:], 0, hid_tiles)
     activate(1)
     project(1)
     if_outer(from_x, 2)
-    if_inner(near_own, 2)
-    expand(3, early[3], 0, hid_tiles)
-    send_x(1)
+    if_outer(send_x, 1)
+    if_outer(send_mix, 0)
+    if_outer(expand_early, 3)
     if_inner(near_own, 1)
     if_inner(near_other, 1)
     if_outer(near_other, 2)
-    expand(2, late[2], 0, hid_tiles)
+    expand(2, late[2], 0, half)
+    if_inner(send_x, 1)
+    expand(2, late[2], half, hid_tiles)
     activate(2)
     if_inner(from_x, 2)
     project(2)
+    if_inner(near_own, 2)
+    if_inner(expand_early, 3)
     if_outer(near_own, 1)
     if_outer(near_other, 1)
+    if_inner(send_x, 2)
     if_inner(near_other, 2)
     expand(3, late[3], 0, half)
-    send_x(2)
+    if_outer(send_x, 2)
     expand(3, late[3], half, hid_tiles)
     activate(3)
     if_outer(send_z, 1)
     project(3)
     if_inner(send_z, 1)
     send_x(3)
+    if_inner(send_mix, 0)
     send_z(2)
+    send_z(3)
     send_z(0)
-    send_mix(0)
     finish_mix(1)
     result = share(0)
-    send_z(3)
+    left(sb, 0)
+    left(xg.at[pl.ds(0, 2)], 1)
+    left(ps, 2)
+    left(xs, 3)
+    left(ps_m, 5)
+
+    @pl.when(z < 3)
+    def _():
+        halo_copy.wait_send()
+
     returned(3)
     result = result + share(3)
     finish_mix(0)
@@ -604,26 +621,8 @@
         result = result + share(k)
     exp_out[...] = result.astype(bf16)
 
-    @pl.when(z < 3)
-    def _():
-        halo_copy.wait_send()
-
-    for k in (1, 2, 3):
-        for p in range(2):
-            if k > 1:
-                forward(0, t, k, p).wait_send()
-            forward(1, t, k, p).wait_send()
-            forward(2, across, k, p).wait_send()
-            r_z(k, p).wait_send()
-    for k in range(4):
-        for p in range(2):
-            d_z(k, p).wait_send()
-            r_x(k, p).wait_send()
-            r_p(p, k).wait_send()
-    for h in range(2):
-        m_p(h, 0).wait_send()
-        m_p(h, 1).wait_send()
-        m_x(h).wait_send()
+    left(xs_m, 6)
+    left(zs.at[pl.ds(1, 3)], 4)
 
 
 def store_kernel(mix_ref, exp_ref, mix_hbm, exp_hbm, sem):
@@ -698,19 +697,15 @@
             pltpu.VMEM((4, cap, quarter), bf16),
             pltpu.VMEM((4, cap, quarter), bf16),
             pltpu.VMEM((4, cap, quarter), bf16),
-            dma((2 * hid_tiles + 9,)),
+            dma((5,)),
             dma((6,)),
-            dma((4, 2)),
-            dma((4, 2)),
-            dma((3, 4, 2)),
-            dma((3, 4, 2)),
+            dma((7,)),
+            dma((4, pieces)),
+            dma((4, pieces)),
             dma((2, 4)),
             dma((2, 4)),
-            dma((4, 2)),
-            dma((4, 2)),
-            dma((4, 2)),
-            dma((4, 2)),
-            dma((2, 3)),
+            dma((4, pieces)),
+            dma((4,)),
             dma((2, 3)),
             dma((2,)),
         ],

time: 35 us -> 33.9 us (0.969)
  Pallas kernels: 34.2 us -> 33.1 us
    pallas_call x1, Pallas kernels: 33.5 us -> 32.3 us  [fused(): pl.pallas_call(fused_kernel, out_shape=(pltpu.VMEM((rows_mix, quarter), b...]
where the time goes in v4:
time: 33.9 us; the launch traced here: 33.7 us
  Pallas kernels  33.1 us (98%)
  between operations  0.64 us (2%)
    pallas_call x1, Pallas kernels, fused(): pl.pallas_call(fused_kernel, out_shape=(pltpu.VMEM((rows_mix, quarter), b...  32.3 us
    pallas_call x1, Pallas kernels, fused(): pl.pallas_call(store_kernel, out_shape=(jax.ShapeDtypeStruct((rows_mix, q...  0.76 us

profile of v4, /device:TPU:0, one launch (start us, length us, event | category | flops | bytes accessed | tf_op | source)
XLA Modules:
  0.0 33.7 jit_solution(4629701177379666778)
XLA Ops:
  0.6 32.3 %shard_map.122 = (bf16[256,512]{1,0:T(8,128)(2,1)S(1)}, bf16[128,512]{1,0:T(8,128)(2,1)S(1)}) custom-call(bf16[128,2048]{1,0:T(8,128)(2,1)} %x_hbm.1, f32[1,2048]{1,0:T(1,128)} %bitcast.4, s32[2,128]{1,0:T(2,128)} %bitcast.6, f32[2,128]{1,0:T(2,128)} %bitcast.7, bf16[256,512]{1,0:T(8,128)(2,1)} %mix_hbm.1, f32[1,2048]{1,0:T(1,128)} %bitcast.5, ...), custom_call_target="tpu_custom_call" | custom-call | tf_op jit(solution)/shard_map/pallas_call | solution.py:662
  32.9 0.8 %shard_map.123 = (bf16[256,512]{1,0:T(8,128)(2,1)}, bf16[128,512]{1,0:T(8,128)(2,1)}) custom-call(bf16[256,512]{1,0:T(8,128)(2,1)S(1)} %get-tuple-element.4.mix_ref, bf16[128,512]{1,0:T(8,128)(2,1)S(1)} %get-tuple-element.5.exp_ref), custom_call_target="tpu_custom_call" | custom-call | tf_op jit(solution)/shard_map/pallas_call | solution.py:728

commit v5 on v4

--- a/solution.py
+++ b/solution.py
@@ -244,6 +244,11 @@
         (mix_hbm, mix_ref),
         (gain_hbm, gain_ref),
     )
+    part = tokens // 4
+    load_x = [
+        pltpu.make_async_copy(x_hbm.at[pl.ds(i * part, part)], x_ref.at[pl.ds(i * part, part)], i_sem.at[2])
+        for i in range(4)
+    ]
     load_i = [pltpu.make_async_copy(src, dst, i_sem.at[i]) for i, (src, dst) in enumerate(pairs)]
     front = (hid_tiles + 1) // 2
     loads = []
@@ -270,7 +275,7 @@
     def loaded(ref, i):
         pltpu.make_async_copy(ref, ref, w_sem.at[i]).wait()
 
-    for c in load_i:
+    for c in load_i[:2] + load_x + load_i[3:]:
         c.start()
 
     def remote(src, dst, send, recv, who):
@@ -326,11 +331,11 @@
             places[k], block, (((0,), (0,)), ((), ())), preferred_element_type=f32
         ).astype(bf16)
 
-    def if_inner(step, k):
-        pl.when(inner == 1)(lambda: step(k))
-
-    def if_outer(step, k):
-        pl.when(inner == 0)(lambda: step(k))
+    def if_inner(step, *k):
+        pl.when(inner == 1)(lambda: step(*k))
+
+    def if_outer(step, *k):
+        pl.when(inner == 0)(lambda: step(*k))
 
     own_cols = xn[t]
     for k in (2, 3):
@@ -382,7 +387,7 @@
     def forward(i, q, slot, p):
         rows = pl.ds(p * piece, piece)
         block = xg.at[q, slot, rows]
-        landed = f_recv.at[slot, p] if i == 0 else g_recv.at[i - 1, slot]
+        landed = f_recv.at[slot - 2, p] if i == 0 else g_recv.at[i - 1, slot - 1]
         return remote(block, block, s_sem.at[1], landed, {"tp": across if i == 0 else near})
 
     def from_z(k):
@@ -406,11 +411,11 @@
 
     def near_own(k):
         block = xg.at[near, k]
-        remote(block, block, s_sem.at[1], g_recv.at[0, k], {"tp": near}).wait_recv()
+        remote(block, block, s_sem.at[1], g_recv.at[0, k - 1], {"tp": near}).wait_recv()
 
     def near_other(k):
         block = xg.at[diagonal, k]
-        remote(block, block, s_sem.at[1], g_recv.at[1, k], {"tp": near}).wait_recv()
+        remote(block, block, s_sem.at[1], g_recv.at[1, k - 1], {"tp": near}).wait_recv()
 
     def mix_half(h):
         rows = slice(h * half_mix, (h + 1) * half_mix)
@@ -468,8 +473,8 @@
                 total = part if total is None else total + part
             gu[k, n] = total
 
-    def expand_early(k):
-        expand(k, early[k], 0, hid_tiles)
+    def expand_early(k, first, last):
+        expand(k, early[k], first, last)
 
     def activate(k):
         for i in range(hid_tiles):
@@ -491,12 +496,12 @@
             zs.at[k, rows],
             zr.at[homes[k], rows],
             s_sem.at[4],
-            z_recv.at[homes[k]],
+            z_recv.at[homes[k] - 1],
             {"ep": home_of[k]},
         )
 
-    def project(k):
-        for i, q in enumerate((diagonal, near, across, t)):
+    def project(k, first=0, last=4):
+        for i, q in list(enumerate((diagonal, near, across, t)))[first:last]:
             part = jnp.dot(hid[k], wd[q], preferred_element_type=f32)
             if i < 2:
                 ps[i, k] = part.astype(bf16)
@@ -504,7 +509,8 @@
                 keep[i - 2, k] = part
             if i == 0:
                 r_p(0, k).start()
-        r_p(1, k).start()
+        if last == 4:
+            r_p(1, k).start()
 
     def send_x(k):
         r_p(0, k).wait_recv()
@@ -528,7 +534,7 @@
         return shares[k] * jnp.dot(places[k], block, preferred_element_type=f32)
 
     def returned(k):
-        remote(zs.at[k], zr.at[k], s_sem.at[4], z_recv.at[k], {"ep": peers[k]}).wait_recv()
+        remote(zs.at[k], zr.at[k], s_sem.at[4], z_recv.at[k - 1], {"ep": peers[k]}).wait_recv()
 
     def left(ref, i):
         remote(ref, ref, s_sem.at[i], s_sem.at[i], {"tp": near}).wait_send()
@@ -559,21 +565,22 @@
     expand(1, early[1], 0, hid_tiles)
     if_outer(from_z, 2)
     if_outer(from_x, 3)
+    if_inner(from_x, 3)
     from_z(1)
     if_inner(from_z, 2)
-    if_inner(from_x, 3)
     expand(1, late[1][:1], 0, hid_tiles)
     if_outer(near_own, 2)
+    if_outer(send_mix, 0)
     expand(2, early[2], 0, hid_tiles)
-    send_x(0)
+    if_inner(send_x, 0)
     near_other(3)
     expand(1, late[1][1:], 0, hid_tiles)
     activate(1)
     project(1)
     if_outer(from_x, 2)
     if_outer(send_x, 1)
-    if_outer(send_mix, 0)
-    if_outer(expand_early, 3)
+    if_outer(send_x, 0)
+    if_outer(expand_early, 3, 0, hid_tiles)
     if_inner(near_own, 1)
     if_inner(near_other, 1)
     if_outer(near_other, 2)
@@ -581,25 +588,32 @@
     if_inner(send_x, 1)
     expand(2, late[2], half, hid_tiles)
     activate(2)
+    project(2, 0, 2)
     if_inner(from_x, 2)
-    project(2)
+    project(2, 2, 4)
     if_inner(near_own, 2)
-    if_inner(expand_early, 3)
+    if_inner(expand_early, 3, 0, half)
+    if_inner(send_x, 2)
+    if_inner(expand_early, 3, half, hid_tiles)
     if_outer(near_own, 1)
     if_outer(near_other, 1)
-    if_inner(send_x, 2)
     if_inner(near_other, 2)
     expand(3, late[3], 0, half)
     if_outer(send_x, 2)
     expand(3, late[3], half, hid_tiles)
     activate(3)
     if_outer(send_z, 1)
+    if_inner(send_z, 1, 0, 1)
     project(3)
-    if_inner(send_z, 1)
+    if_inner(send_z, 1, 1, pieces)
     send_x(3)
+    if_outer(send_z, 2, 0, 1)
+    if_outer(send_z, 3, 0, 1)
+    if_outer(send_z, 2, 1, pieces)
+    if_outer(send_z, 3, 1, pieces)
+    if_inner(send_z, 2)
     if_inner(send_mix, 0)
-    send_z(2)
-    send_z(3)
+    if_inner(send_z, 3)
     send_z(0)
     finish_mix(1)
     result = share(0)
@@ -701,11 +715,11 @@
             dma((6,)),
             dma((7,)),
             dma((4, pieces)),
-            dma((4, pieces)),
-            dma((2, 4)),
+            dma((2, pieces)),
+            dma((2, 3)),
             dma((2, 4)),
             dma((4, pieces)),
-            dma((4,)),
+            dma((3,)),
             dma((2, 3)),
             dma((2,)),
         ],

time: 33.9 us -> 33.8 us (level)
  no operation moved by 1% of the time
where the time goes in v5:
time: 33.8 us; the launch traced here: 33.7 us
  Pallas kernels  33 us (98%)
  between operations  0.64 us (2%)
    pallas_call x1, Pallas kernels, fused(): pl.pallas_call(fused_kernel, out_shape=(pltpu.VMEM((rows_mix, quarter), b...  32.3 us
    pallas_call x1, Pallas kernels, fused(): pl.pallas_call(store_kernel, out_shape=(jax.ShapeDtypeStruct((rows_mix, q...  0.76 us

profile of v5, /device:TPU:0, one launch (start us, length us, event | category | flops | bytes accessed | tf_op | source)
XLA Modules:
  0.0 33.7 jit_solution(7238941351963564003)
XLA Ops:
  0.6 32.3 %shard_map.122 = (bf16[256,512]{1,0:T(8,128)(2,1)S(1)}, bf16[128,512]{1,0:T(8,128)(2,1)S(1)}) custom-call(bf16[128,2048]{1,0:T(8,128)(2,1)} %x_hbm.1, f32[1,2048]{1,0:T(1,128)} %bitcast.4, s32[2,128]{1,0:T(2,128)} %bitcast.6, f32[2,128]{1,0:T(2,128)} %bitcast.7, bf16[256,512]{1,0:T(8,128)(2,1)} %mix_hbm.1, f32[1,2048]{1,0:T(1,128)} %bitcast.5, ...), custom_call_target="tpu_custom_call" | custom-call | tf_op jit(solution)/shard_map/pallas_call | solution.py:676
  32.9 0.8 %shard_map.123 = (bf16[256,512]{1,0:T(8,128)(2,1)}, bf16[128,512]{1,0:T(8,128)(2,1)}) custom-call(bf16[256,512]{1,0:T(8,128)(2,1)S(1)} %get-tuple-element.4.mix_ref, bf16[128,512]{1,0:T(8,128)(2,1)S(1)} %get-tuple-element.5.exp_ref), custom_call_target="tpu_custom_call" | custom-call | tf_op jit(solution)/shard_map/pallas_call | solution.py:742

commit v6 on v5

--- a/solution.py
+++ b/solution.py
@@ -322,9 +322,8 @@
         c.start()
     floated = x_ref[...].astype(f32)
     scale = lax.rsqrt(jnp.mean(floated * floated, axis=1, keepdims=True) + epsilon)
-    xn_val = (floated * scale * norm_ref[...]).astype(bf16)
-    for k in range(4):
-        xn[k] = xn_val[:, k * quarter : (k + 1) * quarter]
+    own_at = pl.ds(pl.multiple_of(t * quarter, quarter), quarter)
+    own_cols = (x_ref[:, own_at].astype(f32) * scale * norm_ref[:, own_at]).astype(bf16)
 
     def gathered(k, block):
         return lax.dot_general(
@@ -337,7 +336,6 @@
     def if_outer(step, *k):
         pl.when(inner == 0)(lambda: step(*k))
 
-    own_cols = xn[t]
     for k in (2, 3):
         sb[k] = gathered(k, own_cols)
     for c in load_i[4:]:
@@ -372,6 +370,9 @@
 
     if_outer(send_rows, (2, 3))
     if_inner(send_rows, (3, 2))
+    xn_val = (floated * scale * norm_ref[...]).astype(bf16)
+    for k in range(4):
+        xn[k] = xn_val[:, k * quarter : (k + 1) * quarter]
     sb[0] = gathered(1, own_cols)
     sb[1] = gathered(1, xn[across])
     send_rows((0, 1))

time: 33.8 us -> 33.8 us (level)
  no operation moved by 1% of the time
where the time goes in v6:
time: 33.8 us; the launch traced here: 33.6 us
  Pallas kernels  33 us (98%)
  between operations  0.64 us (2%)
    pallas_call x1, Pallas kernels, fused(): pl.pallas_call(fused_kernel, out_shape=(pltpu.VMEM((rows_mix, quarter), b...  32.2 us
    pallas_call x1, Pallas kernels, fused(): pl.pallas_call(store_kernel, out_shape=(jax.ShapeDtypeStruct((rows_mix, q...  0.76 us

profile of v6, /device:TPU:0, one launch (start us, length us, event | category | flops | bytes accessed | tf_op | source)
XLA Modules:
  0.0 33.6 jit_solution(5989056274598767632)
XLA Ops:
  0.6 32.2 %shard_map.122 = (bf16[256,512]{1,0:T(8,128)(2,1)S(1)}, bf16[128,512]{1,0:T(8,128)(2,1)S(1)}) custom-call(bf16[128,2048]{1,0:T(8,128)(2,1)} %x_hbm.1, f32[1,2048]{1,0:T(1,128)} %bitcast.4, s32[2,128]{1,0:T(2,128)} %bitcast.6, f32[2,128]{1,0:T(2,128)} %bitcast.7, bf16[256,512]{1,0:T(8,128)(2,1)} %mix_hbm.1, f32[1,2048]{1,0:T(1,128)} %bitcast.5, ...), custom_call_target="tpu_custom_call" | custom-call | tf_op jit(solution)/shard_map/pallas_call | solution.py:677
  32.9 0.8 %shard_map.123 = (bf16[256,512]{1,0:T(8,128)(2,1)}, bf16[128,512]{1,0:T(8,128)(2,1)}) custom-call(bf16[256,512]{1,0:T(8,128)(2,1)S(1)} %get-tuple-element.4.mix_ref, bf16[128,512]{1,0:T(8,128)(2,1)S(1)} %get-tuple-element.5.exp_ref), custom_call_target="tpu_custom_call" | custom-call | tf_op jit(solution)/shard_map/pallas_call | solution.py:743
